TPU v7x, 128 devices: a whole 4x4x4 slice. The times are simulated.
128 devices in a mesh: sp: 16 (over z, x), dp: 8 (over y, core).
Axes of the slice: x: 4, y: 4, z: 4, core: 2. Of those that a mesh axis runs over, the one named last changes fastest.
Arguments:
- hidden_in: bfloat16 [8, 2048, 2048], P('dp', 'sp'), may hold values from -6 to 6
- mix_cotangent: bfloat16 [8, 2048, 4096], P('dp', 'sp'), may hold values from -0.119628906 to 0.119628906
- query_weight: bfloat16 [2048, 4096], P('dp', 'sp'), may hold values from -0.125 to 0.125
- key_weight: bfloat16 [2048, 4096], P('dp', 'sp'), may hold values from -0.125 to 0.125
- value_weight: bfloat16 [2048, 4096], P('dp', 'sp'), may hold values from -0.125 to 0.125
- decay_log: float32 [16], P('sp'), may hold values from -0.034 to -0.000146484375, as said below
Outputs:
- grad_hidden: bfloat16 [8, 2048, 2048], P('dp', 'sp')
- grad_query: float32 [2048, 4096], P('dp', 'sp')
- grad_key: float32 [2048, 4096], P('dp', 'sp')
- grad_value: float32 [2048, 4096], P('dp', 'sp')
Inputs may be any that keep to these rules, and one draw needn't show every extreme that they name: Each head's decay_log is negative.
All inputs are finite; a program needn't handle non-finite values.
Results may differ from a plain program's by a relative error of at most 0.015.
Values may be sent and summed in bfloat16 or wider, within the bound.
A program may use at most 64 MiB of HBM per device.

v0:
```python
import jax
import jax.numpy as jnp
from jax import lax
from jax.sharding import PartitionSpec as P

BLOCK = 128


def in_blocks(array, dim, size):
    shape = array.shape
    pieces = array.reshape(*shape[:dim], size, shape[dim] // size, *shape[dim + 1 :])
    return jnp.moveaxis(pieces, dim, 0)


def sent_and_summed(array, axis, dim):
    pieces = in_blocks(array, dim, lax.axis_size(axis))
    arrived = lax.all_to_all(pieces, axis, split_axis=0, concat_axis=0, tiled=True)
    return arrived.astype(jnp.float32).sum(axis=0)


def head_grads(queries, key_rows, values, cotangent, log_rate):
    length = queries.shape[0]
    head_dim = queries.shape[1]
    blocks = length // BLOCK
    scale = head_dim ** (-0.5)
    keys_scaled = (key_rows.astype(jnp.float32) * scale).astype(jnp.bfloat16)
    offsets = jnp.arange(BLOCK, dtype=jnp.float32)
    spread = offsets[:, None] - offsets[None, :]
    inner_decay = jnp.where(spread >= 0, jnp.exp(log_rate * jnp.maximum(spread, 0.0)), 0.0)
    query_decay = jnp.exp(log_rate * (offsets + 1.0))
    key_decay = jnp.exp(log_rate * (BLOCK - 1.0 - offsets))
    block_decay = jnp.exp(log_rate * BLOCK)

    def split_blocks(series):
        return series.reshape(blocks, BLOCK, series.shape[-1])

    def forward(carried, inputs):
        query_block, key_block, value_block, grad_block = inputs
        mixed = (
            jnp.dot(grad_block, value_block.T, preferred_element_type=jnp.float32) * inner_decay
        ).astype(jnp.bfloat16)
        within = jnp.dot(mixed, key_block, preferred_element_type=jnp.float32)
        across = (
            jnp.dot(grad_block, carried.astype(jnp.bfloat16).T, preferred_element_type=jnp.float32)
            * query_decay[:, None]
        )
        weighted = (key_block.astype(jnp.float32) * key_decay[:, None]).astype(jnp.bfloat16)
        updated = carried * block_decay + jnp.dot(
            weighted.T, value_block, preferred_element_type=jnp.float32
        )
        return (updated, (within + across, mixed))

    def backward(carried, inputs):
        query_block, key_block, value_block, grad_block, mixed = inputs
        scores = (
            jnp.dot(query_block, key_block.T, preferred_element_type=jnp.float32) * inner_decay
        ).astype(jnp.bfloat16)
        state_bf = carried.astype(jnp.bfloat16)
        grad_v = (
            jnp.dot(scores.T, grad_block, preferred_element_type=jnp.float32)
            + jnp.dot(key_block, state_bf, preferred_element_type=jnp.float32) * key_decay[:, None]
        )
        grad_k = (
            jnp.dot(mixed.T, query_block, preferred_element_type=jnp.float32)
            + jnp.dot(value_block, state_bf.T, preferred_element_type=jnp.float32)
            * key_decay[:, None]
        ) * scale
        weighted = (query_block.astype(jnp.float32) * query_decay[:, None]).astype(jnp.bfloat16)
        updated = carried * block_decay + jnp.dot(
            weighted.T, grad_block, preferred_element_type=jnp.float32
        )
        return (updated, (grad_k, grad_v))

    inputs = (
        split_blocks(queries),
        split_blocks(keys_scaled),
        split_blocks(values),
        split_blocks(cotangent),
    )
    initial = jnp.zeros((head_dim, values.shape[-1]), jnp.float32)
    final_state, (grad_q, mixed_all) = lax.scan(forward, initial, inputs)
    final_back, (grad_k, grad_v) = lax.scan(backward, initial, inputs + (mixed_all,), reverse=True)
    return (grad_q.reshape(length, -1), grad_k.reshape(length, -1), grad_v.reshape(length, -1))


def group_grads(log_rates, queries, key_rows, values, cotangent):
    length = queries.shape[0]
    head_count = log_rates.shape[0]

    def by_head(series):
        return series.reshape(length, head_count, -1).transpose(1, 0, 2)

    def to_rows(series):
        return series.transpose(1, 0, 2).reshape(length, -1)

    grad_q, grad_k, grad_v = jax.vmap(head_grads)(
        by_head(queries), by_head(key_rows), by_head(values), by_head(cotangent), log_rates
    )
    return jnp.concatenate((to_rows(grad_q), to_rows(grad_k), to_rows(grad_v)), axis=1).astype(
        jnp.bfloat16
    )


def body(hidden_in, mix_cotangent, query_weight, key_weight, value_weight, decay_log):
    own_rows = hidden_in[0]
    columns = query_weight.shape[1]
    stacked = jnp.stack((query_weight, key_weight, value_weight), axis=1)
    gathered = lax.all_gather(stacked, "dp", axis=0, tiled=True)
    weights = gathered.reshape(gathered.shape[0], 3 * columns)
    cotangent = lax.all_to_all(mix_cotangent[0], "sp", split_axis=1, concat_axis=0, tiled=True)
    all_rows = lax.all_gather(own_rows, "sp", axis=0, tiled=True)
    projected = jnp.dot(all_rows, weights, preferred_element_type=jnp.float32).astype(jnp.bfloat16)
    gradients = group_grads(
        decay_log,
        projected[:, :columns],
        projected[:, columns : 2 * columns],
        projected[:, 2 * columns :],
        cotangent,
    )
    input_sum = lax.psum_scatter(
        lax.dot_general(
            gradients, weights, (((1,), (1,)), ((), ())), preferred_element_type=jnp.float32
        ).astype(jnp.bfloat16),
        "sp",
        scatter_dimension=0,
        tiled=True,
    )
    grad_hidden = input_sum[None]
    summed = sent_and_summed(
        lax.dot_general(
            all_rows, gradients, (((0,), (0,)), ((), ())), preferred_element_type=jnp.float32
        ).astype(jnp.bfloat16),
        "dp",
        0,
    ) / lax.axis_size("dp")
    return (
        grad_hidden,
        summed[:, :columns],
        summed[:, columns : 2 * columns],
        summed[:, 2 * columns :],
    )


def solution(mesh):
    placed = (
        P("dp", "sp", None),
        P("dp", "sp", None),
        P("dp", "sp"),
        P("dp", "sp"),
        P("dp", "sp"),
        P("sp"),
    )
    return jax.shard_map(
        body,
        mesh=mesh,
        in_specs=placed,
        out_specs=(P("dp", "sp", None), P("dp", "sp"), P("dp", "sp"), P("dp", "sp")),
        check_vma=False,
    )
```

profile of v0, /device:TPU:0, one launch (start us, length us, event | category | flops | bytes accessed | tf_op | source)
XLA Modules:
  0.0 429.9 jit_solution(11572848178626721793)
XLA Ops:
  13.3 8.0 %all-to-all-start = ((bf16[128,16,256]{0,2,1:T(8,128)(2,1)}), bf16[128,16,256]{0,2,1:T(8,128)(2,1)S(1)}, u32[]{:S(2)}, u32[]{:S(2)}) async-start(bf16[128,16,256]{0,2,1:T(8,128)(2,1)} %bitcast.6), calls=%async_computation | async-start | bytes 2097152 | tf_op jit(solution)/shard_map/all_to_all | solution.py:110
  22.0 16.9 %all-to-all-done = bf16[128,16,256]{0,2,1:T(8,128)(2,1)S(1)} async-done(((bf16[128,16,256]{0,2,1:T(8,128)(2,1)}), bf16[128,16,256]{0,2,1:T(8,128)(2,1)S(1)}, u32[]{:S(2)}, u32[]{:S(2)}) %all-to-all-start) | async-done | bytes 1048608 | tf_op jit(solution)/shard_map/all_to_all | solution.py:110
  40.3 4.6 %all-gather.4.cloned.1.call-done = bf16[2048,3,256]{0,2,1:T(8,128)(2,1)} async-done(((bf16[256,3,256]{0,2,1:T(8,128)(2,1)}), bf16[2048,3,256]{0,2,1:T(8,128)(2,1)}) %all-gather.4.cloned.1.call-update) | async-done | bytes 3145744 | tf_op jit(solution)/shard_map/all_gather | solution.py:108
  44.9 74.0 %all-gather.6.cloned.1.call-done = bf16[1,2048,2048]{2,1,0:T(8,128)(2,1)} async-done(((bf16[1,128,2048]{2,1,0:T(8,128)(2,1)}), bf16[1,2048,2048]{2,1,0:T(8,128)(2,1)}) %all-gather.6.cloned.1.call-update) | async-done | bytes 8388624 | tf_op jit(solution)/shard_map/all_gather | solution.py:111
  119.0 10.1 %fusion.112 = bf16[2048,768]{0,1:T(8,128)(2,1)S(1)} fusion(bf16[2048,768]{0,1:T(8,128)(2,1)} %bitcast.220, bf16[1,2048,2048]{2,1,0:T(8,128)(2,1)} %all-gather.6.cloned.1.call-done), kind=kOutput, calls=%fused_computation.113 | convolution fusion | flops 6444023808 | bytes 14680064 | tf_op jit(solution)/shard_map/dot_general | solution.py:112
  133.3 95.3 %while.38 = (s32[]{:T(128)}, f32[1,256,256]{2,1,0:T(8,128)S(1)}, bf16[16,1,128,256]{3,2,1,0:T(8,128)(2,1)}, bf16[16,1,128,128]{3,2,1,0:T(8,128)(2,1)}, f32[1]{0:...) while((s32[]{:T(128)}, f32[1,256,256]{2,1,0:T(8,128)S(1)}, ...), condition=%wide.region_1.2_spmd.clone.clone.clone, body=%wide.region_0.1_spmd.clone.clone.clone.sunk | while | flops 50872832 | bytes 1677952 | solution.py:81
  133.3 2.4 bitcast_dynamic-update-slice_fusion.2
  139.4 2.3 bitcast_dynamic-update-slice_fusion.2
  142.5 1.7 fusion.155
  145.3 2.3 bitcast_dynamic-update-slice_fusion.2
  148.5 1.7 fusion.155
  151.3 2.3 bitcast_dynamic-update-slice_fusion.2
  157.2 2.3 bitcast_dynamic-update-slice_fusion.2
  163.2 2.3 bitcast_dynamic-update-slice_fusion.2
  169.1 2.3 bitcast_dynamic-update-slice_fusion.2
  172.3 1.7 fusion.155
  175.1 2.3 bitcast_dynamic-update-slice_fusion.2
  181.0 2.3 bitcast_dynamic-update-slice_fusion.2
  187.0 2.3 bitcast_dynamic-update-slice_fusion.2
  192.9 2.3 bitcast_dynamic-update-slice_fusion.2
  198.9 2.3 bitcast_dynamic-update-slice_fusion.2
  204.8 2.3 bitcast_dynamic-update-slice_fusion.2
  208.0 1.7 fusion.155
  210.8 2.3 bitcast_dynamic-update-slice_fusion.2
  216.7 2.3 bitcast_dynamic-update-slice_fusion.2
  222.7 2.3 bitcast_dynamic-update-slice_fusion.2
  225.8 1.7 fusion.155
  230.2 96.6 %while.39 = (s32[]{:T(128)}, f32[1,256,256]{2,1,0:T(8,128)S(1)}, bf16[16,1,128,256]{3,2,1,0:T(8,128)(2,1)S(1)}, bf16[16,1,128,256]{3,2,1,0:T(8,128)(2,1)S(1)}, f...) while((s32[]{:T(128)}, f32[1,256,256]{2,1,0:T(8,128)S(1)}, ...), condition=%wide.region_3.4_spmd.clone.clone.clone, body=%wide.region_2.3_spmd.clone.clone.clone.sunk | while | flops 76202496 | bytes 2402974 | solution.py:82
  230.2 1.9 fusion.170
  236.2 1.9 fusion.170
  242.2 1.9 fusion.170
  248.3 1.9 fusion.170
  254.3 1.9 fusion.170
  260.3 1.9 fusion.170
  266.4 1.9 fusion.170
  272.4 1.9 fusion.170
  278.5 1.9 fusion.170
  284.5 1.9 fusion.170
  290.5 1.9 fusion.170
  296.6 1.9 fusion.170
  302.6 1.9 fusion.170
  308.6 1.9 fusion.170
  314.7 1.9 fusion.170
  320.7 1.9 fusion.170
  326.7 10.9 %convolution_convert_fusion = bf16[2048,2048]{1,0:T(8,128)(2,1)} fusion(bf16[2048,768]{0,1:T(8,128)(2,1)} %bitcast.221, bf16[2048,256]{1,0:T(8,128)(2,1)S(1)} %bitcast.213, bf16[2048,256]{1,0:T(8,128)(2,1)S(1)} %bitcast.211, bf16[2048,256]{1,0:T(8,128)(2,1)} %bitcast.215), kind=kOutput, calls=%fused_computation.107 | convolution fusion | flops 6456082432 | bytes 14680064 | tf_op jit(solution)/shard_map/dot_general | solution.py:121
  338.8 9.1 %fusion.106 = bf16[768,2048]{1,0:T(8,128)(2,1)S(1)} fusion(bf16[1,2048,2048]{2,1,0:T(8,128)(2,1)} %all-gather.6.cloned.1.call-done, bf16[2048,256]{1,0:T(8,128)(2,1)S(1)} %bitcast.214, bf16[2048,256]{1,0:T(8,128)(2,1)S(1)} %bitcast.212, bf16[2048,256]{1,0:T(8,128)(2,1)S(1)} %bitcast.216), kind=kOutput, calls=%fused_computation.109 | convolution fusion | flops 6453460992 | bytes 14680064 | tf_op jit(solution)/shard_map/dot_general | solution.py:130
  348.2 42.5 %all_to_all.21 = bf16[8,256,768]{1,2,0:T(8,128)(2,1)S(1)} all-to-all(bf16[8,256,768]{1,2,0:T(8,128)(2,1)S(1)} %bitcast.205), channel_id=1, replica_groups=mesh['sp'=16,'dp'=8] {'dp'}, dimensions={0} | all-to-all | bytes 6291456 | tf_op jit(solution)/shard_map/all_to_all | solution.py:17
  393.8 29.6 %reduce-scatter.2.cloned.1.call-done = bf16[128,2048]{1,0:T(8,128)(2,1)} async-done(((bf16[2048,2048]{1,0:T(8,128)(2,1)}), bf16[128,2048]{1,0:T(8,128)(2,1)}) %reduce-scatter.2.cloned.1.call-update) | async-done | bytes 524304 | tf_op jit(solution)/shard_map/reduce_scatter | solution.py:120
  (175 shorter events, 132.6 us)
Async XLA Ops:
  7.2 4.7 %copy-start.1 = (bf16[1,128,4096]{2,1,0:T(8,128)(2,1)S(1)}, bf16[1,128,4096]{2,1,0:T(8,128)(2,1)}, u32[]{:S(2)}) copy-start(bf16[1,128,4096]{2,1,0:T(8,128)(2,1)} %param.11) | copy-start | bytes 3145732
  7.2 37.7 %all-gather.4.cloned.1.call-start = ((), (), s32[]{:S(2)}) async-start(), calls=%async_computation.3 | async-start | bytes 3538944 | tf_op jit(solution)/shard_map/all_gather | solution.py:108
  11.2 107.8 %all-gather.6.cloned.1.call-start = ((), (), s32[]{:S(2)}) async-start(), calls=%async_computation.5 | async-start | bytes 8912896 | tf_op jit(solution)/shard_map/all_gather | solution.py:111
  13.3 25.7 %all-to-all-start = ((bf16[128,16,256]{0,2,1:T(8,128)(2,1)}), bf16[128,16,256]{0,2,1:T(8,128)(2,1)S(1)}, u32[]{:S(2)}, u32[]{:S(2)}) async-start(bf16[128,16,256]{0,2,1:T(8,128)(2,1)} %bitcast.6), calls=%async_computation | async-start | bytes 2097152 | tf_op jit(solution)/shard_map/all_to_all | solution.py:110
  21.3 402.1 %reduce-scatter.2.cloned.1.call-start = ((), (), s32[]{:S(2)}) async-start(), calls=%async_computation.4 | async-start | bytes 8912896 | tf_op jit(solution)/shard_map/reduce_scatter | solution.py:120
  133.3 95.3 %copy-start = (bf16[2048,256]{0,1:T(8,128)(2,1)S(1)}, bf16[2048,256]{0,1:T(8,128)(2,1)}, u32[]{:S(2)}) copy-start(bf16[2048,256]{0,1:T(8,128)(2,1)} %get-tuple-element.631) | copy-start | bytes 3145732
  337.6 1.2 copy-start.2
Sparse Core Ops, SparseCore 0:
  11.3 33.5 all-gather.3
  47.1 71.8 all-gather.5
  337.7 85.5 reduce-scatter.1
where the time goes:
time: 436 us; the launch traced here: 430 us
  matrix products  199 us (46%)
  waiting for transfers between devices  126 us (29%)
  blocking collectives  42.5 us (10%)
  other arithmetic  22.6 us (5%)
  local copies, waits for them, and re-layouts  15.4 us (4%)
  between operations  14.6 us (3%)
  starting transfers between devices  8.11 us (2%)
    all_gather x1, waiting for transfers between devices, body(): all_rows = lax.all_gather(own_rows, 'sp', axis=0, tiled=True)  74 us
    all_to_all x1, blocking collectives, sent_and_summed(): lax.all_to_all(pieces, axis, split_axis=0, concat_axis=0, tiled=True)  42.5 us
    dot_general x16, matrix products, forward(): jnp.dot(grad_block, value_block.T, preferred_element_type=jnp.float32)  37.1 us
    dot_general x16, matrix products, backward(): jnp.dot(scores.T, grad_block, preferred_element_type=jnp.float32)  30.2 us
    reduce_scatter x1, waiting for transfers between devices, body(): lax.psum_scatter(lax.dot_general(gradients, weights, (((1,), (1,)), ((),...  29.6 us
    dot_general x16, matrix products, forward(): jnp.dot(grad_block, carried.astype(jnp.bfloat16).T, preferred_element_typ...  26.8 us
    dot_general x16, matrix products, backward(): jnp.dot(weighted.T, grad_block, preferred_element_type=jnp.float32)  18.6 us
    dot_general x16, matrix products, forward(): jnp.dot(weighted.T, value_block, preferred_element_type=jnp.float32)  18 us
  transfers between devices with their start and end apart: 4, of which 4 were waited for; matrix products, arithmetic and copies ran while one was open for 4% of the time, Pallas kernels for 0%

commit v1 on v0

v1 whole, which is shorter than its diff:
```python
import functools

import jax
import jax.numpy as jnp
from jax import lax
from jax.experimental import pallas as pl
from jax.experimental.pallas import tpu as pltpu
from jax.sharding import PartitionSpec as P

BLOCK = 128
F32 = jnp.float32
BF16 = jnp.bfloat16


def dot(a, b):
    return lax.dot_general(a, b, (((1,), (0,)), ((), ())), preferred_element_type=F32)


def dot_t(a, b):
    return lax.dot_general(a, b, (((1,), (1,)), ((), ())), preferred_element_type=F32)


def t_dot(a, b):
    return lax.dot_general(a, b, (((0,), (0,)), ((), ())), preferred_element_type=F32)


def rows_of(block):
    return pl.ds(pl.multiple_of(block * BLOCK, BLOCK), BLOCK)


def make_decays(rate, inner_ref, inner_t_ref, query_ref, key_ref):
    row = lax.broadcasted_iota(jnp.int32, (BLOCK, BLOCK), 0)
    col = lax.broadcasted_iota(jnp.int32, (BLOCK, BLOCK), 1)
    spread = (row - col).astype(F32)
    inner_ref[...] = jnp.where(spread >= 0, jnp.exp(rate * jnp.maximum(spread, 0.0)), 0.0)
    inner_t_ref[...] = jnp.where(spread <= 0, jnp.exp(rate * jnp.maximum(-spread, 0.0)), 0.0)
    offset = lax.broadcasted_iota(jnp.int32, query_ref.shape, 0).astype(F32)
    query_ref[...] = jnp.exp(rate * (offset + 1.0))
    key_ref[...] = jnp.exp(rate * (BLOCK - 1.0 - offset))


def in_block(block, head, scale, qkv, cot, decays, grads, fwd_states, bwd_states):
    inner_ref, inner_t_ref, query_ref, key_ref = decays
    rows = rows_of(block)
    queries = qkv[rows, 0:head]
    keys = qkv[rows, head : 2 * head]
    values = qkv[rows, 2 * head : 3 * head]
    given = cot[rows, :]
    mixed = (dot_t(given, values) * inner_ref[...]).astype(BF16)
    grads[rows, 0:head] = dot(mixed, keys)
    mixed_t = (dot_t(values, given) * inner_t_ref[...]).astype(BF16)
    grads[rows, head : 2 * head] = dot(mixed_t, queries) * scale
    scores_t = (dot_t(keys, queries) * inner_t_ref[...]).astype(BF16)
    grads[rows, 2 * head : 3 * head] = dot(scores_t, given)
    keys_w = (keys.astype(F32) * key_ref[...]).astype(BF16)
    fwd_states[block] = t_dot(keys_w, values)
    queries_w = (queries.astype(F32) * query_ref[...]).astype(BF16)
    bwd_states[block] = t_dot(queries_w, given)


def run_states(rate, blocks, fwd_states, bwd_states, fwd_bf, bwd_bf):
    step = jnp.exp(jnp.full(fwd_states.shape[1:], BLOCK, F32) * rate)

    def forward(i, carried):
        fwd_bf[i] = carried.astype(BF16)
        return carried * step + fwd_states[i]

    lax.fori_loop(0, blocks, forward, jnp.zeros(fwd_states.shape[1:], F32))

    def backward(n, carried):
        i = blocks - 1 - n
        bwd_bf[i] = carried.astype(BF16)
        return carried * step + bwd_states[i]

    lax.fori_loop(0, blocks, backward, jnp.zeros(fwd_states.shape[1:], F32))


def cross_block(block, head, scale, qkv, cot, decays, grads, fwd_bf, bwd_bf, out):
    _, _, query_ref, key_ref = decays
    rows = rows_of(block)
    keys = qkv[rows, head : 2 * head]
    values = qkv[rows, 2 * head : 3 * head]
    state = fwd_bf[block]
    back = bwd_bf[block]
    grad_q = grads[rows, 0:head] + dot_t(cot[rows, :], state) * query_ref[...]
    grad_k = grads[rows, head : 2 * head] + dot_t(values, back) * (key_ref[...] * scale)
    grad_v = grads[rows, 2 * head : 3 * head] + dot(keys, back) * key_ref[...]
    out[rows, 0:head] = grad_q.astype(BF16)
    out[rows, head : 2 * head] = grad_k.astype(BF16)
    out[rows, 2 * head : 3 * head] = grad_v.astype(BF16)


def mixer_kernel(rate_ref, rows_ref, weight_ref, cot_ref, out_ref, qkv, grads, inner, inner_t, query_d, key_d, fwd, bwd, fwd_bf, bwd_bf):
    length, wide = out_ref.shape
    head = wide // 3
    blocks = length // BLOCK
    scale = head ** (-0.5)
    rate = rate_ref[0]
    decays = (inner, inner_t, query_d, key_d)
    make_decays(rate, *decays)

    def project(n, _):
        rows = rows_of(n)
        got = dot(rows_ref[rows, :], weight_ref[...])
        qkv[rows, 0:head] = got[:, 0:head].astype(BF16)
        qkv[rows, head : 2 * head] = (got[:, head : 2 * head].astype(BF16).astype(F32) * scale).astype(BF16)
        qkv[rows, 2 * head : 3 * head] = got[:, 2 * head : 3 * head].astype(BF16)
        return _

    lax.fori_loop(0, blocks, project, 0)

    def inside(n, _):
        in_block(n, head, scale, qkv, cot_ref, decays, grads, fwd, bwd)
        return _

    lax.fori_loop(0, blocks, inside, 0)
    run_states(rate, blocks, fwd, bwd, fwd_bf, bwd_bf)

    def across(n, _):
        cross_block(n, head, scale, qkv, cot_ref, decays, grads, fwd_bf, bwd_bf, out_ref)
        return _

    lax.fori_loop(0, blocks, across, 0)


def mixer(rate, rows, weights, cot):
    length = rows.shape[0]
    wide = weights.shape[1]
    head = wide // 3
    blocks = length // BLOCK
    vmem = pl.BlockSpec(memory_space=pltpu.VMEM)
    return pl.pallas_call(
        mixer_kernel,
        out_shape=jax.ShapeDtypeStruct((length, wide), BF16),
        in_specs=[pl.BlockSpec(memory_space=pltpu.SMEM), vmem, vmem, vmem],
        out_specs=vmem,
        scratch_shapes=[
            pltpu.VMEM((length, wide), BF16),
            pltpu.VMEM((length, wide), F32),
            pltpu.VMEM((BLOCK, BLOCK), F32),
            pltpu.VMEM((BLOCK, BLOCK), F32),
            pltpu.VMEM((BLOCK, head), F32),
            pltpu.VMEM((BLOCK, head), F32),
            pltpu.VMEM((blocks, head, head), F32),
            pltpu.VMEM((blocks, head, head), F32),
            pltpu.VMEM((blocks, head, head), BF16),
            pltpu.VMEM((blocks, head, head), BF16),
        ],
        compiler_params=pltpu.CompilerParams(vmem_limit_bytes=56 * 1024 * 1024),
        cost_estimate=pl.CostEstimate(flops=9 * 10**9, bytes_accessed=20 * 10**6, transcendentals=0),
    )(rate, rows, weights, cot)


def in_blocks(array, dim, size):
    shape = array.shape
    pieces = array.reshape(*shape[:dim], size, shape[dim] // size, *shape[dim + 1 :])
    return jnp.moveaxis(pieces, dim, 0)


def sent_and_summed(array, axis, dim):
    pieces = in_blocks(array, dim, lax.axis_size(axis))
    arrived = lax.all_to_all(pieces, axis, split_axis=0, concat_axis=0, tiled=True)
    return arrived.astype(F32).sum(axis=0)


def body(hidden_in, mix_cotangent, query_weight, key_weight, value_weight, decay_log):
    own_rows = hidden_in[0]
    columns = query_weight.shape[1]
    stacked = jnp.concatenate((query_weight, key_weight, value_weight), axis=1)
    weights = lax.all_gather(stacked, "dp", axis=0, tiled=True)
    cotangent = lax.all_to_all(mix_cotangent[0], "sp", split_axis=1, concat_axis=0, tiled=True)
    all_rows = lax.all_gather(own_rows, "sp", axis=0, tiled=True)
    gradients = mixer(decay_log, all_rows, weights, cotangent)
    input_sum = lax.psum_scatter(
        lax.dot_general(gradients, weights, (((1,), (1,)), ((), ())), preferred_element_type=F32).astype(BF16),
        "sp",
        scatter_dimension=0,
        tiled=True,
    )
    summed = sent_and_summed(
        lax.dot_general(all_rows, gradients, (((0,), (0,)), ((), ())), preferred_element_type=F32).astype(BF16), "dp", 0
    ) / lax.axis_size("dp")
    return (input_sum[None], summed[:, :columns], summed[:, columns : 2 * columns], summed[:, 2 * columns :])


def solution(mesh):
    placed = (P("dp", "sp", None), P("dp", "sp", None), P("dp", "sp"), P("dp", "sp"), P("dp", "sp"), P("sp"))
    return jax.shard_map(
        body,
        mesh=mesh,
        in_specs=placed,
        out_specs=(P("dp", "sp", None), P("dp", "sp"), P("dp", "sp"), P("dp", "sp")),
        check_vma=False,
    )
```

time: 436 us -> 247 us (0.57); the launches traced: 430 us -> 246 us
  matrix products: 199 us -> 20 us
  Pallas kernels: 0 us -> 29.6 us
  other arithmetic: 22.6 us -> 2.3 us
  local copies, waits for them, and re-layouts: 15.4 us -> 7.46 us
    dot_general x145 -> x0, matrix products: 179 us -> none  [the longest x16 37.1 us: forward(): jnp.dot(grad_block, value_block.T, preferred_element_type=jnp.float32)]
    pallas_call x0 -> x1, Pallas kernels: none -> 29.6 us  [mixer(): pl.pallas_call(mixer_kernel, out_shape=jax.ShapeDtypeStruct((length, wide...]
    mul x32 -> x0, other arithmetic: 21.1 us -> none  [the longest x16 10.6 us: backward(): jnp.dot(value_block, state_bf.T, preferred_element_type=jnp.float32)]
    unnamed x17 -> x10, local copies, waits for them, and re-layouts: 12.7 us -> 5.86 us
  transfers between devices with their start and end apart: 4 -> 4, of which waited for: 4 -> 4; matrix products, arithmetic and copies ran while one was open for 4% -> 6% of each run, Pallas kernels for 0% -> 0%
where the time goes in v1:
time: 247 us; the launch traced here: 246 us
  waiting for transfers between devices  122 us (49%)
  blocking collectives  42.5 us (17%)
  Pallas kernels  29.6 us (12%)
  matrix products  20 us (8%)
  between operations  14.5 us (6%)
  starting transfers between devices  8.11 us (3%)
  local copies, waits for them, and re-layouts  7.46 us (3%)
    all_gather x1, waiting for transfers between devices, body(): all_rows = lax.all_gather(own_rows, 'sp', axis=0, tiled=True)  73 us
    all_to_all x1, blocking collectives, sent_and_summed(): lax.all_to_all(pieces, axis, split_axis=0, concat_axis=0, tiled=True)  42.5 us
    pallas_call x1, Pallas kernels, mixer(): pl.pallas_call(mixer_kernel, out_shape=jax.ShapeDtypeStruct((length, wide...  29.6 us
    reduce_scatter x1, waiting for transfers between devices, body(): lax.psum_scatter(lax.dot_general(gradients, weights, (((1,), (1,)), ((),...  29 us
    all_to_all x1, waiting for transfers between devices, body(): lax.all_to_all(mix_cotangent[0], 'sp', split_axis=1, concat_axis=0, tiled...  17 us
    dot_general x1, matrix products, body(): lax.dot_general(gradients, weights, (((1,), (1,)), ((), ())), preferred_e...  10.8 us
    dot_general x1, matrix products, body(): lax.dot_general(all_rows, gradients, (((0,), (0,)), ((), ())), preferred_...  9.14 us
    all_to_all x1, starting transfers between devices, body(): lax.all_to_all(mix_cotangent[0], 'sp', split_axis=1, concat_axis=0, tiled...  7.99 us
  transfers between devices with their start and end apart: 4, of which 4 were waited for; matrix products, arithmetic and copies ran while one was open for 6% of the time, Pallas kernels for 0%

profile of v1, /device:TPU:0, one launch (start us, length us, event | category | flops | bytes accessed | tf_op | source)
XLA Modules:
  0.0 246.3 jit_solution(13824161050726542052)
XLA Ops:
  7.2 0.0 all-gather.4.cloned.1.call-start
  7.2 1.8 pad_maximum_fusion
  9.0 0.0 all-gather.4.cloned.1.call-update
  9.0 0.0 all-gather.6.cloned.1.call-start
  9.1 0.7 all-gather.6.cloned.1.call-update
  9.8 1.5 copy.19
  11.3 1.3 copy.11
  12.6 8.0 %all-to-all-start = ((bf16[128,16,256]{2,0,1:T(8,128)(2,1)}), bf16[128,16,256]{2,0,1:T(8,128)(2,1)S(1)}, u32[]{:S(2)}, u32[]{:S(2)}) async-start(bf16[128,16,256]{2,0,1:T(8,128)(2,1)} %copy.11), calls=%async_computation | async-start | bytes 2097152 | tf_op jit(solution)/shard_map/all_to_all | solution.py:171
  20.6 0.0 reduce-scatter.2.cloned.1.call-start
  21.3 17.0 %all-to-all-done = bf16[128,16,256]{2,0,1:T(8,128)(2,1)S(1)} async-done(((bf16[128,16,256]{2,0,1:T(8,128)(2,1)}), bf16[128,16,256]{2,0,1:T(8,128)(2,1)S(1)}, u32[]{:S(2)}, u32[]{:S(2)}) %all-to-all-start) | async-done | bytes 1048608 | tf_op jit(solution)/shard_map/all_to_all | solution.py:171
  38.3 0.0 copy-start
  38.3 2.2 all-gather.4.cloned.1.call-done.weight_ref
  40.5 73.0 %all-gather.6.cloned.1.call-done = bf16[1,2048,2048]{2,1,0:T(8,128)(2,1)} async-done(((bf16[1,128,2048]{2,1,0:T(8,128)(2,1)}), bf16[1,2048,2048]{2,1,0:T(8,128)(2,1)}) %all-gather.6.cloned.1.call-update) | async-done | bytes 8388624 | tf_op jit(solution)/shard_map/all_gather | solution.py:172
  113.5 0.0 copy-done
  113.5 0.0 copy-start.1
  113.5 29.6 %shard_map.93 = bf16[2048,768]{1,0:T(8,128)(2,1)} custom-call(f32[1]{0:T(128)S(6)} %copy.22.rate_ref, bf16[2048,2048]{1,0:T(8,128)(2,1)} %bitcast.23, bf16[2048,768]{1,0:T(8,128)(2,1)} %all-gather.4.cloned.1.call-done.weight_ref, bf16[2048,256]{1,0:T(8,128)(2,1)} %bitcast.22), custom_call_target="tpu_custom_call" | custom-call | flops 8999999488 | bytes 20000000 | tf_op jit(solution)/shard_map/pallas_call | solution.py:132
  143.1 0.0 copy-done.1
  143.1 10.8 %convolution_convert_fusion = bf16[2048,2048]{1,0:T(8,128)(2,1)} fusion(bf16[2048,768]{1,0:T(8,128)(2,1)} %shard_map.93, bf16[2048,768]{1,0:T(8,128)(2,1)S(1)} %copy-done.1), kind=kOutput, calls=%fused_computation | convolution fusion | flops 6446645248 | bytes 14680064 | tf_op jit(solution)/shard_map/dot_general | solution.py:175
  153.9 0.0 copy-start.2
  153.9 0.0 reduce-scatter.2.cloned.1.call-update
  153.9 1.9 copy-done.2
  155.8 9.1 %convolution_convert_fusion.1 = bf16[768,2048]{1,0:T(8,128)(2,1)S(1)} fusion(bf16[2048,768]{1,0:T(8,128)(2,1)S(1)} %copy-done.2, bf16[1,2048,2048]{2,1,0:T(8,128)(2,1)} %all-gather.6.cloned.1.call-done), kind=kOutput, calls=%fused_computation.2 | convolution fusion | flops 6444023808 | bytes 14680064 | tf_op jit(solution)/shard_map/dot_general | solution.py:181
  165.0 0.2 copy.21
  165.2 42.5 %all_to_all.24 = bf16[8,256,768]{1,2,0:T(8,128)(2,1)S(1)} all-to-all(bf16[8,256,768]{1,2,0:T(8,128)(2,1)S(1)} %bitcast.18), channel_id=1, replica_groups=mesh['sp'=16,'dp'=8] {'dp'}, dimensions={0} | all-to-all | bytes 6291456 | tf_op jit(solution)/shard_map/all_to_all | solution.py:162
  207.7 0.4 convert_reduce_fusion
  208.2 0.1 broadcast_multiply_fusion
  208.2 0.1 fusion.1
  208.3 0.8 copy.16
  209.1 0.8 copy.15
  209.9 0.8 copy.14
  210.8 29.0 %reduce-scatter.2.cloned.1.call-done = bf16[128,2048]{1,0:T(8,128)(2,1)} async-done(((bf16[2048,2048]{1,0:T(8,128)(2,1)}), bf16[128,2048]{1,0:T(8,128)(2,1)}) %reduce-scatter.2.cloned.1.call-update) | async-done | bytes 524304 | tf_op jit(solution)/shard_map/reduce_scatter | solution.py:174
Async XLA Ops:
  7.2 33.3 %all-gather.4.cloned.1.call-start = ((), (), s32[]{:S(2)}) async-start(), calls=%async_computation.3 | async-start | bytes 3538944 | tf_op jit(solution)/shard_map/all_gather | solution.py:170
  9.0 104.5 %all-gather.6.cloned.1.call-start = ((), (), s32[]{:S(2)}) async-start(), calls=%async_computation.5 | async-start | bytes 8912896 | tf_op jit(solution)/shard_map/all_gather | solution.py:172
  12.6 25.7 %all-to-all-start = ((bf16[128,16,256]{2,0,1:T(8,128)(2,1)}), bf16[128,16,256]{2,0,1:T(8,128)(2,1)S(1)}, u32[]{:S(2)}, u32[]{:S(2)}) async-start(bf16[128,16,256]{2,0,1:T(8,128)(2,1)} %copy.11), calls=%async_computation | async-start | bytes 2097152 | tf_op jit(solution)/shard_map/all_to_all | solution.py:171
  20.6 219.1 %reduce-scatter.2.cloned.1.call-start = ((), (), s32[]{:S(2)}) async-start(), calls=%async_computation.4 | async-start | bytes 8912896 | tf_op jit(solution)/shard_map/reduce_scatter | solution.py:174
  38.3 75.2 %copy-start = (bf16[128,16,256]{2,0,1:T(8,128)(2,1)}, bf16[128,16,256]{2,0,1:T(8,128)(2,1)S(1)}, u32[]{:S(2)}) copy-start(bf16[128,16,256]{2,0,1:T(8,128)(2,1)S(1)} %all-to-all-done) | copy-start | bytes 3145732
  113.5 29.6 %copy-start.1 = (bf16[2048,768]{1,0:T(8,128)(2,1)S(1)}, bf16[2048,768]{1,0:T(8,128)(2,1)}, u32[]{:S(2)}) copy-start(bf16[2048,768]{1,0:T(8,128)(2,1)} %all-gather.4.cloned.1.call-done.weight_ref) | copy-start | bytes 9437188
  153.9 1.9 copy-start.2
Sparse Core Ops, SparseCore 0:
  10.2 30.1 all-gather.3
  42.6 70.8 all-gather.5
  154.1 85.6 reduce-scatter.1

commit v2 on v1

--- a/solution.py
+++ b/solution.py
@@ -1,5 +1,3 @@
-import functools
-
 import jax
 import jax.numpy as jnp
 from jax import lax
@@ -8,8 +6,13 @@
 from jax.sharding import PartitionSpec as P
 
 BLOCK = 128
+HALF = 64
+PART = 32
+RING = 4
 F32 = jnp.float32
 BF16 = jnp.bfloat16
+MESH = pl.DeviceIdType.MESH
+SIDES = (1, -1)
 
 
 def dot(a, b):
@@ -26,6 +29,20 @@
 
 def rows_of(block):
     return pl.ds(pl.multiple_of(block * BLOCK, BLOCK), BLOCK)
+
+
+def pick(index, values):
+    got = jnp.int32(values[-1])
+    for place, value in enumerate(values[:-1]):
+        got = jnp.where(index == place, jnp.int32(value), got)
+    return got
+
+
+def add_into(target, rows, others):
+    total = target[rows, :].astype(F32)
+    for other in others:
+        total = total + other.astype(F32)
+    target[rows, :] = total.astype(BF16)
 
 
 def make_decays(rate, inner_ref, inner_t_ref, query_ref, key_ref):
@@ -90,52 +107,421 @@
     out[rows, 2 * head : 3 * head] = grad_v.astype(BF16)
 
 
-def mixer_kernel(rate_ref, rows_ref, weight_ref, cot_ref, out_ref, qkv, grads, inner, inner_t, query_d, key_d, fwd, bwd, fwd_bf, bwd_bf):
-    length, wide = out_ref.shape
-    head = wide // 3
-    blocks = length // BLOCK
+def all_kernel(
+    rate_ref,
+    own_x,
+    own_cot,
+    wq_ref,
+    wk_ref,
+    wv_ref,
+    out_x,
+    out_q,
+    out_k,
+    out_v,
+    xall,
+    w,
+    qkv,
+    cot,
+    grads,
+    inner,
+    inner_t,
+    query_d,
+    key_d,
+    fwd,
+    bwd,
+    fwd_bf,
+    bwd_bf,
+    g,
+    part,
+    first1,
+    first2,
+    second1,
+    second2,
+    wg,
+    pair1,
+    ring1,
+    ring2,
+    local_sem,
+    send_sem,
+    recv_sem,
+):
+    depth = xall.shape[1]
+    head = cot.shape[1]
+    blocks = RING * RING
     scale = head ** (-0.5)
+    sp = lax.axis_index("sp")
+    dp = lax.axis_index("dp")
+    z, x = lax.div(sp, RING), lax.rem(sp, RING)
+    y, core = lax.div(dp, 2), lax.rem(dp, 2)
     rate = rate_ref[0]
     decays = (inner, inner_t, query_d, key_d)
+    names = {}
+    sent = []
+
+    def slot(*name):
+        return names.setdefault(name, len(names))
+
+    def wrap(value):
+        return lax.rem(value + RING, RING)
+
+    def block_at(dz, dx):
+        return wrap(z + dz) * RING + wrap(x + dx)
+
+    def plane(dz, dx):
+        return (block_at(dz, dx), dp)
+
+    def along_y(dy):
+        return (sp, wrap(y + dy) * 2 + core)
+
+    partner = (sp, y * 2 + 1 - core)
+
+    def along(half, first, second):
+        return (second, first) if half == 0 else (first, second)
+
+    def copy(index, source, target, device):
+        return pltpu.make_async_remote_copy(
+            src_ref=source,
+            dst_ref=target,
+            send_sem=send_sem.at[index],
+            recv_sem=recv_sem.at[index],
+            device_id=device,
+            device_id_type=MESH,
+        )
+
+    def send(index, source, target, device):
+        copy(index, source, target, device).start()
+        sent.append((index, source))
+
+    def arrived(index, target):
+        copy(index, target, target, partner).wait_recv()
+
+    barrier = pltpu.get_barrier_semaphore()
+    friends = [plane(dz, dx) for dz in range(RING) for dx in range(RING) if dz or dx]
+    friends = friends + [along_y(1), along_y(-1), partner]
+    for friend in friends:
+        pl.semaphore_signal(barrier, inc=1, device_id=friend, device_id_type=MESH)
+
+    own_rows = rows_of(sp)
+    w_rows = pl.ds(pl.multiple_of(dp * head, head), head)
+    loads = [
+        pltpu.make_async_copy(own_x.at[0], xall.at[own_rows, :], local_sem.at[0]),
+        pltpu.make_async_copy(wq_ref, w.at[w_rows, 0:head], local_sem.at[1]),
+        pltpu.make_async_copy(wk_ref, w.at[w_rows, head : 2 * head], local_sem.at[2]),
+        pltpu.make_async_copy(wv_ref, w.at[w_rows, 2 * head : 3 * head], local_sem.at[3]),
+        pltpu.make_async_copy(
+            own_cot.at[0, :, pl.ds(pl.multiple_of(sp * head, head), head)], cot.at[own_rows, :], local_sem.at[4]
+        ),
+    ]
+    for load in loads:
+        load.start()
     make_decays(rate, *decays)
-
-    def project(n, _):
-        rows = rows_of(n)
-        got = dot(rows_ref[rows, :], weight_ref[...])
+    for load in loads:
+        load.wait()
+    pl.semaphore_wait(barrier, len(friends))
+
+    def x_rows(block, start, count):
+        return xall.at[pl.ds(pl.multiple_of(block * BLOCK + start, PART), count), :]
+
+    def part_start(half, side):
+        return half * HALF + (0 if side == 1 else PART)
+
+    def gather_block(half, p, q):
+        return block_at(*along(half, p, q))
+
+    def gather_send(name, half, p, q, side, axis):
+        block = gather_block(half, p, q)
+        if name[0] in ("s1", "s2"):
+            rows = x_rows(block, half * HALF, HALF)
+        else:
+            rows = x_rows(block, part_start(half, side), PART)
+        device = plane(*along(half, side, 0)) if axis == 0 else plane(*along(half, 0, side))
+        send(slot(*name), rows, rows, device)
+
+    def gather_wait(name, half, p, q, side):
+        block = gather_block(half, p, q)
+        if name[0] in ("s1", "s2"):
+            rows = x_rows(block, half * HALF, HALF)
+        else:
+            rows = x_rows(block, part_start(half, side), PART)
+        arrived(slot(*name), rows)
+
+    def w_part(dy, which, start, count):
+        first = (wrap(y + dy) * 2 + which) * head
+        return w.at[pl.ds(pl.multiple_of(first + start, BLOCK), count), :]
+
+    for half in range(2):
+        for side in SIDES:
+            gather_send(("s1", half, side), half, 0, 0, side, 0)
+    for side in SIDES:
+        send(slot("w1", side), w_part(0, core, 0, head), w_part(0, core, 0, head), along_y(side))
+    send(slot("wc", 0), w_part(0, core, 0, head), w_part(0, core, 0, head), partner)
+    for half in range(2):
+        for side in SIDES:
+            gather_send(("s2", half, 0, side), half, 0, 0, side, 1)
+    for offset in A2A_ORDER:
+        target = lax.rem(sp + offset, blocks)
+        send(
+            slot("cot", offset),
+            own_cot.at[0, :, pl.ds(pl.multiple_of(target * head, head), head)],
+            cot.at[own_rows, :],
+            (target, dp),
+        )
+
+    def project(block):
+        rows = rows_of(block)
+        got = dot(xall[rows, :], w[...])
         qkv[rows, 0:head] = got[:, 0:head].astype(BF16)
         qkv[rows, head : 2 * head] = (got[:, head : 2 * head].astype(BF16).astype(F32) * scale).astype(BF16)
         qkv[rows, 2 * head : 3 * head] = got[:, 2 * head : 3 * head].astype(BF16)
-        return _
-
-    lax.fori_loop(0, blocks, project, 0)
-
-    def inside(n, _):
-        in_block(n, head, scale, qkv, cot_ref, decays, grads, fwd, bwd)
-        return _
-
-    lax.fori_loop(0, blocks, inside, 0)
+
+    def inside(block):
+        in_block(block, head, scale, qkv, cot, decays, grads, fwd, bwd)
+
+    def loop(places, *works):
+        def step(n, carried):
+            block = block_at(pick(n, [dz for dz, _ in places]), pick(n, [dx for _, dx in places]))
+            for work in works:
+                work(block)
+            return carried
+
+        lax.fori_loop(0, len(places), step, 0)
+
+    near = [(0, 0), (0, 1), (0, 3), (1, 0), (3, 0)]
+    corners = [(1, 1), (1, 3), (3, 1), (3, 3)]
+    far = [(0, 2), (2, 0)]
+    edges = [(1, 2), (3, 2), (2, 1), (2, 3)]
+    last = [(2, 2)]
+
+    for half in range(2):
+        for side in SIDES:
+            gather_wait(("s1", half, side), half, -side, 0, side)
+            gather_send(("f1", half, side), half, -side, 0, side, 0)
+    for half in range(2):
+        for near_p in SIDES:
+            for side in SIDES:
+                gather_send(("s2", half, near_p, side), half, near_p, 0, side, 1)
+
+    for side in SIDES:
+        arrived(slot("w1", side), w_part(-side, core, 0, head))
+        rows = w_part(-side, core, 0 if side == 1 else BLOCK, BLOCK)
+        send(slot("w2", side), rows, rows, along_y(side))
+        rows = w_part(-side, core, 0, head)
+        send(slot("wc", side), rows, rows, partner)
+
+    for half in range(2):
+        for side in SIDES:
+            gather_wait(("s2", half, 0, side), half, 0, -side, side)
+            gather_send(("f2", half, 0, side), half, 0, -side, side, 1)
+
+    for side in SIDES:
+        arrived(slot("w2", side), w_part(2, core, 0 if side == 1 else BLOCK, BLOCK))
+    send(slot("wc", 2), w_part(2, core, 0, head), w_part(2, core, 0, head), partner)
+    for dy in (0, 1, -1, 2):
+        arrived(slot("wc", dy), w_part(-dy, 1 - core, 0, head))
+
+    loop(near, project)
+
+    for half in range(2):
+        for side in SIDES:
+            gather_wait(("f1", half, side), half, 2, 0, side)
+    for half in range(2):
+        for side in SIDES:
+            gather_send(("s2", half, 2, side), half, 2, 0, side, 1)
+
+    for offset in A2A_ORDER:
+        arrived(slot("cot", offset), cot.at[rows_of(lax.rem(sp + blocks - offset, blocks)), :])
+    loop(near, inside)
+
+    for near_p in SIDES:
+        for half in range(2):
+            for side in SIDES:
+                gather_wait(("s2", half, near_p, side), half, near_p, -side, side)
+                gather_send(("f2", half, near_p, side), half, near_p, -side, side, 1)
+    loop(corners, project, inside)
+
+    for half in range(2):
+        for side in SIDES:
+            gather_wait(("f2", half, 0, side), half, 0, 2, side)
+    loop(far, project, inside)
+
+    for half in range(2):
+        for side in SIDES:
+            gather_wait(("s2", half, 2, side), half, 2, -side, side)
+            gather_send(("f2", half, 2, side), half, 2, -side, side, 1)
+
+    for near_p in SIDES:
+        for half in range(2):
+            for side in SIDES:
+                gather_wait(("f2", half, near_p, side), half, near_p, 2, side)
+    loop(edges, project, inside)
+
+    for half in range(2):
+        for side in SIDES:
+            gather_wait(("f2", half, 2, side), half, 2, 2, side)
+    loop(last, project, inside)
+
     run_states(rate, blocks, fwd, bwd, fwd_bf, bwd_bf)
 
-    def across(n, _):
-        cross_block(n, head, scale, qkv, cot_ref, decays, grads, fwd_bf, bwd_bf, out_ref)
-        return _
-
-    lax.fori_loop(0, blocks, across, 0)
-
-
-def mixer(rate, rows, weights, cot):
-    length = rows.shape[0]
-    wide = weights.shape[1]
-    head = wide // 3
-    blocks = length // BLOCK
+    def finish(block):
+        cross_block(block, head, scale, qkv, cot, decays, grads, fwd_bf, bwd_bf, g)
+        rows = rows_of(block)
+        part[rows, :] = dot_t(g[rows, :], w[...]).astype(BF16)
+
+    def sum_block(half, f, q):
+        return block_at(*((f, q) if half == 0 else (q, f)))
+
+    def sum_rows(block, start, count):
+        return pl.ds(pl.multiple_of(block * BLOCK + start, PART), count)
+
+    def f_device(half, side):
+        return plane(side, 0) if half == 0 else plane(0, side)
+
+    def g_device(half, side):
+        return plane(0, side) if half == 0 else plane(side, 0)
+
+    def which(side):
+        return 0 if side == 1 else 1
+
+    def send_first(half, j):
+        for side in SIDES:
+            rows = sum_rows(sum_block(half, 2, j), part_start(half, side), PART)
+            send(slot("F1", half, j, side), part.at[rows, :], first1.at[half, which(side), j], f_device(half, side))
+
+    def send_second(half, j):
+        for side in SIDES:
+            block = sum_block(half, side, j)
+            rows = sum_rows(block, part_start(half, side), PART)
+            arrived(slot("F1", half, j, side), first1.at[half, which(side), j])
+            add_into(part, rows, [first1[half, which(side), j]])
+        for side in SIDES:
+            block = sum_block(half, side, j)
+            rows = sum_rows(block, half * HALF, HALF)
+            send(slot("F2", half, j, side), part.at[rows, :], first2.at[half, which(side), j], f_device(half, side))
+
+    def take_second(half, j):
+        for side in SIDES:
+            arrived(slot("F2", half, j, side), first2.at[half, which(side), j])
+        rows = sum_rows(sum_block(half, 0, j), half * HALF, HALF)
+        add_into(part, rows, [first2[half, 0, j], first2[half, 1, j]])
+
+    loop([(2, 2), (2, 1), (2, 3), (2, 0)], finish)
+    for j in (2, 1, 3, 0):
+        send_first(0, j)
+    send_first(1, 2)
+    loop([(1, 2), (3, 2), (0, 2)], finish)
+    for j in (1, 3, 0):
+        send_first(1, j)
+    loop(corners, finish)
+    for half in range(2):
+        send_second(half, 2)
+    loop([(1, 0), (3, 0), (0, 1), (0, 3), (0, 0)], finish)
+    for j in (1, 3, 0):
+        for half in range(2):
+            send_second(half, j)
+
+    def weight_part(chunk):
+        columns = pl.ds(pl.multiple_of(chunk * head, head), head)
+        wg[chunk] = t_dot(xall[:, columns], g[...]).astype(BF16)
+
+    ahead = (2, 1, 3, 0)
+
+    def others(n, carried):
+        weight_part(wrap(y + pick(n, ahead)) * 2 + 1 - core)
+        return carried
+
+    lax.fori_loop(0, RING, others, 0)
+    for n in range(RING):
+        chunk = wrap(y + ahead[n]) * 2 + 1 - core
+        send(slot("pair", n), wg.at[chunk], pair1.at[n], partner)
+
+    for half in range(2):
+        take_second(half, 2)
+    for half in range(2):
+        for side in SIDES:
+            rows = sum_rows(sum_block(half, 0, 2), part_start(half, side), PART)
+            send(slot("G1", half, side), part.at[rows, :], second1.at[half, which(side)], g_device(half, side))
+
+    def mine(n, carried):
+        weight_part(wrap(y + pick(n, ahead)) * 2 + core)
+        return carried
+
+    lax.fori_loop(0, RING, mine, 0)
+    for n in range(RING):
+        chunk = wrap(y + ahead[n]) * 2 + core
+        arrived(slot("pair", n), pair1.at[n])
+        wg[chunk] = (wg[chunk].astype(F32) + pair1[n].astype(F32)).astype(BF16)
+        if n == 0:
+            for side in SIDES:
+                rows = pl.ds(0 if side == 1 else BLOCK, BLOCK)
+                send(slot("Y1", side), wg.at[chunk, rows, :], ring1.at[which(side)], along_y(side))
+
+    for j in (1, 3):
+        for half in range(2):
+            take_second(half, j)
+
+    for side in SIDES:
+        chunk = wrap(y + side) * 2 + core
+        rows = pl.ds(0 if side == 1 else BLOCK, BLOCK)
+        arrived(slot("Y1", side), ring1.at[which(side)])
+        wg[chunk, rows, :] = (wg[chunk, rows, :].astype(F32) + ring1[which(side)].astype(F32)).astype(BF16)
+        send(slot("Y2", side), wg.at[chunk], ring2.at[which(side)], along_y(side))
+
+    for half in range(2):
+        for side in SIDES:
+            block = sum_block(half, 0, side)
+            arrived(slot("G1", half, side), second1.at[half, which(side)])
+            add_into(part, sum_rows(block, part_start(half, side), PART), [second1[half, which(side)]])
+            rows = sum_rows(block, half * HALF, HALF)
+            send(slot("G2", half, side), part.at[rows, :], second2.at[half, which(side)], g_device(half, side))
+
+    for half in range(2):
+        take_second(half, 0)
+
+    for side in SIDES:
+        arrived(slot("Y2", side), ring2.at[which(side)])
+    total = (wg[y * 2 + core].astype(F32) + ring2[0].astype(F32) + ring2[1].astype(F32)) * (1.0 / (2 * RING))
+    out_q[...] = total[:, 0:head]
+    out_k[...] = total[:, head : 2 * head]
+    out_v[...] = total[:, 2 * head : 3 * head]
+
+    for half in range(2):
+        for side in SIDES:
+            arrived(slot("G2", half, side), second2.at[half, which(side)])
+        rows = sum_rows(sp, half * HALF, HALF)
+        total = part[rows, :].astype(F32) + second2[half, 0].astype(F32) + second2[half, 1].astype(F32)
+        out_x[0, half * HALF : (half + 1) * HALF, :] = total.astype(BF16)
+
+    for index, source in sent:
+        copy(index, source, source, partner).wait_send()
+
+
+A2A_ORDER = (1, 15, 4, 12, 3, 5, 11, 13, 2, 14, 8, 6, 7, 9, 10)
+COPIES = 160
+
+
+def body(hidden_in, mix_cotangent, query_weight, key_weight, value_weight, decay_log):
+    depth = hidden_in.shape[2]
+    head = query_weight.shape[1]
+    blocks = RING * RING
+    length = blocks * BLOCK
+    wide = 3 * head
     vmem = pl.BlockSpec(memory_space=pltpu.VMEM)
+    anywhere = pl.BlockSpec(memory_space=pl.ANY)
     return pl.pallas_call(
-        mixer_kernel,
-        out_shape=jax.ShapeDtypeStruct((length, wide), BF16),
-        in_specs=[pl.BlockSpec(memory_space=pltpu.SMEM), vmem, vmem, vmem],
-        out_specs=vmem,
+        all_kernel,
+        out_shape=(
+            jax.ShapeDtypeStruct(hidden_in.shape, BF16),
+            jax.ShapeDtypeStruct((head, head), F32),
+            jax.ShapeDtypeStruct((head, head), F32),
+            jax.ShapeDtypeStruct((head, head), F32),
+        ),
+        in_specs=[pl.BlockSpec(memory_space=pltpu.SMEM)] + [anywhere] * 5,
+        out_specs=(vmem,) * 4,
         scratch_shapes=[
+            pltpu.VMEM((length, depth), BF16),
+            pltpu.VMEM((depth, wide), BF16),
             pltpu.VMEM((length, wide), BF16),
+            pltpu.VMEM((length, head), BF16),
             pltpu.VMEM((length, wide), F32),
             pltpu.VMEM((BLOCK, BLOCK), F32),
             pltpu.VMEM((BLOCK, BLOCK), F32),
@@ -145,42 +531,25 @@
             pltpu.VMEM((blocks, head, head), F32),
             pltpu.VMEM((blocks, head, head), BF16),
             pltpu.VMEM((blocks, head, head), BF16),
+            pltpu.VMEM((length, wide), BF16),
+            pltpu.VMEM((length, depth), BF16),
+            pltpu.VMEM((2, 2, RING, PART, depth), BF16),
+            pltpu.VMEM((2, 2, RING, HALF, depth), BF16),
+            pltpu.VMEM((2, 2, PART, depth), BF16),
+            pltpu.VMEM((2, 2, HALF, depth), BF16),
+            pltpu.VMEM((2 * RING, depth // (2 * RING), wide), BF16),
+            pltpu.VMEM((RING, depth // (2 * RING), wide), BF16),
+            pltpu.VMEM((2, depth // (4 * RING), wide), BF16),
+            pltpu.VMEM((2, depth // (2 * RING), wide), BF16),
+            pltpu.SemaphoreType.DMA((5,)),
+            pltpu.SemaphoreType.DMA((COPIES,)),
+            pltpu.SemaphoreType.DMA((COPIES,)),
         ],
-        compiler_params=pltpu.CompilerParams(vmem_limit_bytes=56 * 1024 * 1024),
-        cost_estimate=pl.CostEstimate(flops=9 * 10**9, bytes_accessed=20 * 10**6, transcendentals=0),
-    )(rate, rows, weights, cot)
-
-
-def in_blocks(array, dim, size):
-    shape = array.shape
-    pieces = array.reshape(*shape[:dim], size, shape[dim] // size, *shape[dim + 1 :])
-    return jnp.moveaxis(pieces, dim, 0)
-
-
-def sent_and_summed(array, axis, dim):
-    pieces = in_blocks(array, dim, lax.axis_size(axis))
-    arrived = lax.all_to_all(pieces, axis, split_axis=0, concat_axis=0, tiled=True)
-    return arrived.astype(F32).sum(axis=0)
-
-
-def body(hidden_in, mix_cotangent, query_weight, key_weight, value_weight, decay_log):
-    own_rows = hidden_in[0]
-    columns = query_weight.shape[1]
-    stacked = jnp.concatenate((query_weight, key_weight, value_weight), axis=1)
-    weights = lax.all_gather(stacked, "dp", axis=0, tiled=True)
-    cotangent = lax.all_to_all(mix_cotangent[0], "sp", split_axis=1, concat_axis=0, tiled=True)
-    all_rows = lax.all_gather(own_rows, "sp", axis=0, tiled=True)
-    gradients = mixer(decay_log, all_rows, weights, cotangent)
-    input_sum = lax.psum_scatter(
-        lax.dot_general(gradients, weights, (((1,), (1,)), ((), ())), preferred_element_type=F32).astype(BF16),
-        "sp",
-        scatter_dimension=0,
-        tiled=True,
-    )
-    summed = sent_and_summed(
-        lax.dot_general(all_rows, gradients, (((0,), (0,)), ((), ())), preferred_element_type=F32).astype(BF16), "dp", 0
-    ) / lax.axis_size("dp")
-    return (input_sum[None], summed[:, :columns], summed[:, columns : 2 * columns], summed[:, 2 * columns :])
+        compiler_params=pltpu.CompilerParams(
+            vmem_limit_bytes=67043328, collective_id=0, has_side_effects=True
+        ),
+        cost_estimate=pl.CostEstimate(flops=21 * 10**9, bytes_accessed=4 * 10**6, transcendentals=0),
+    )(decay_log, hidden_in, mix_cotangent, query_weight, key_weight, value_weight)
 
 
 def solution(mesh):

time: 247 us -> 129 us (0.52)
  waiting for transfers between devices: 122 us -> 0 us
  Pallas kernels: 29.6 us -> 123 us
  blocking collectives: 42.5 us -> 0 us
  matrix products: 20 us -> 0 us
  between operations: 14.5 us -> 1.3 us
  starting transfers between devices: 8.11 us -> 0 us
  local copies, waits for them, and re-layouts: 7.46 us -> 4.72 us
    pallas_call x1, Pallas kernels: 29.6 us -> 123 us  [body(): pl.pallas_call(all_kernel, out_shape=(jax.ShapeDtypeStruct(hidden_in.shap...]
    all_gather x2 -> x0, waiting for transfers between devices: 75.2 us -> none  [the longest x1 73 us: body(): all_rows = lax.all_gather(own_rows, 'sp', axis=0, tiled=True)]
    all_to_all x1 -> x0, blocking collectives: 42.5 us -> none  [sent_and_summed(): lax.all_to_all(pieces, axis, split_axis=0, concat_axis=0, tiled=True)]
    reduce_scatter x1 -> x0, waiting for transfers between devices: 29 us -> none  [body(): lax.psum_scatter(lax.dot_general(gradients, weights, (((1,), (1,)), ((),...]
    dot_general x2 -> x0, matrix products: 20 us -> none  [the longest x1 10.8 us: body(): lax.dot_general(gradients, weights, (((1,), (1,)), ((), ())), preferred_e...]
    all_to_all x1 -> x0, waiting for transfers between devices: 17 us -> none  [body(): lax.all_to_all(mix_cotangent[0], 'sp', split_axis=1, concat_axis=0, tiled...]
    all_to_all x1 -> x0, starting transfers between devices: 7.99 us -> none  [body(): lax.all_to_all(mix_cotangent[0], 'sp', split_axis=1, concat_axis=0, tiled...]
  transfers between devices with their start and end apart: 4 -> 0, of which waited for: 4 -> 0; matrix products, arithmetic and copies ran while one was open for 6% -> 0% of each run, Pallas kernels for 0% -> 0%
where the time goes in v2:
time: 129 us
  Pallas kernels  123 us (95%)
  local copies, waits for them, and re-layouts  4.72 us (4%)
  between operations  1.3 us (1%)
    pallas_call x1, Pallas kernels, body(): pl.pallas_call(all_kernel, out_shape=(jax.ShapeDtypeStruct(hidden_in.shap...  123 us
    unnamed x10, local copies, waits for them, and re-layouts  4.72 us

profile of v2, /device:TPU:0, one launch (start us, length us, event | category | flops | bytes accessed | tf_op | source)
XLA Modules:
  0.0 128.6 jit_solution(12255420978237644031)
XLA Ops:
  1.3 122.6 %shard_map.93 = (bf16[1,128,2048]{2,1,0:T(8,128)(2,1)}, f32[256,256]{1,0:T(8,128)}, f32[256,256]{1,0:T(8,128)}, f32[256,256]{1,0:T(8,128)}) custom-call(f32[1]{0:T(128)S(6)} %copy.14.rate_ref, bf16[1,128,2048]{2,1,0:T(8,128)(2,1)} %own_x.1, bf16[1,128,4096]{2,1,0:T(8,128)(2,1)} %own_cot.1, bf16[256,256]{1,0:T(8,128)(2,1)} %wq_ref.1, ...), custom_call_target="tpu_custom_call" | custom-call | flops 20999999488 | bytes 4000000 | tf_op jit(solution)/shard_map/pallas_call | solution.py:510
  123.9 0.0 copy-start.2
  123.9 1.9 %copy.15 = bf16[1,128,2048]{2,1,0:T(8,128)(2,1)} copy(bf16[1,128,2048]{2,1,0:T(8,128)(2,1)} %get-tuple-element.8) | data formatting | bytes 1048576
  125.8 0.0 copy-done.2
  125.8 0.0 copy-start.1
  125.8 0.7 copy.16
  126.5 0.3 copy-done.1
  126.8 0.0 copy-start
  126.8 0.7 copy.17
  127.6 0.3 copy-done
  127.9 0.7 copy.18
Async XLA Ops:
  123.9 1.9 %copy-start.2 = (f32[256,256]{1,0:T(8,128)S(1)}, f32[256,256]{1,0:T(8,128)}, u32[]{:S(2)}) copy-start(f32[256,256]{1,0:T(8,128)} %get-tuple-element.9) | copy-start | bytes 786436
  125.8 1.0 copy-start.1
  126.8 1.0 copy-start

commit v3 on v2

--- a/solution.py
+++ b/solution.py
@@ -76,20 +76,23 @@
 
 
 def run_states(rate, blocks, fwd_states, bwd_states, fwd_bf, bwd_bf):
-    step = jnp.exp(jnp.full(fwd_states.shape[1:], BLOCK, F32) * rate)
-
-    def forward(i, carried):
-        fwd_bf[i] = carried.astype(BF16)
-        return carried * step + fwd_states[i]
-
-    lax.fori_loop(0, blocks, forward, jnp.zeros(fwd_states.shape[1:], F32))
-
-    def backward(n, carried):
-        i = blocks - 1 - n
-        bwd_bf[i] = carried.astype(BF16)
-        return carried * step + bwd_states[i]
-
-    lax.fori_loop(0, blocks, backward, jnp.zeros(fwd_states.shape[1:], F32))
+    size = 32
+    wide = fwd_states.shape[2]
+    step = jnp.exp(jnp.full((size, wide), BLOCK, F32) * rate)
+
+    def chunk(n, carried):
+        rows = pl.ds(pl.multiple_of(n * size, size), size)
+        ahead = jnp.zeros((size, wide), F32)
+        back = jnp.zeros((size, wide), F32)
+        for i in range(blocks):
+            fwd_bf[i, rows, :] = ahead.astype(BF16)
+            ahead = ahead * step + fwd_states[i, rows, :]
+            last = blocks - 1 - i
+            bwd_bf[last, rows, :] = back.astype(BF16)
+            back = back * step + bwd_states[last, rows, :]
+        return carried
+
+    lax.fori_loop(0, fwd_states.shape[1] // size, chunk, 0)
 
 
 def cross_block(block, head, scale, qkv, cot, decays, grads, fwd_bf, bwd_bf, out):
@@ -115,9 +118,7 @@
     wk_ref,
     wv_ref,
     out_x,
-    out_q,
-    out_k,
-    out_v,
+    out_w,
     xall,
     w,
     qkv,
@@ -161,6 +162,12 @@
     def slot(*name):
         return names.setdefault(name, len(names))
 
+    def slots(count, *name):
+        first = slot(*name, 0)
+        for place in range(1, count):
+            assert slot(*name, place) == first + place
+        return first
+
     def wrap(value):
         return lax.rem(value + RING, RING)
 
@@ -191,6 +198,9 @@
     def send(index, source, target, device):
         copy(index, source, target, device).start()
         sent.append((index, source))
+
+    def send_in_loop(index, source, target, device):
+        copy(index, source, target, device).start()
 
     def arrived(index, target):
         copy(index, target, target, partner).wait_recv()
@@ -289,7 +299,6 @@
     near = [(0, 0), (0, 1), (0, 3), (1, 0), (3, 0)]
     corners = [(1, 1), (1, 3), (3, 1), (3, 3)]
     far = [(0, 2), (2, 0)]
-    edges = [(1, 2), (3, 2), (2, 1), (2, 3)]
     last = [(2, 2)]
 
     for half in range(2):
@@ -353,7 +362,7 @@
         for half in range(2):
             for side in SIDES:
                 gather_wait(("f2", half, near_p, side), half, near_p, 2, side)
-    loop(edges, project, inside)
+        loop([(2, near_p), (near_p, 2)], project, inside)
 
     for half in range(2):
         for side in SIDES:
@@ -382,16 +391,20 @@
     def which(side):
         return 0 if side == 1 else 1
 
+    firsts = {(half, side): slots(RING, "F1", half, side) for half in range(2) for side in SIDES}
+
     def send_first(half, j):
         for side in SIDES:
             rows = sum_rows(sum_block(half, 2, j), part_start(half, side), PART)
-            send(slot("F1", half, j, side), part.at[rows, :], first1.at[half, which(side), j], f_device(half, side))
+            send_in_loop(
+                firsts[half, side] + j, part.at[rows, :], first1.at[half, which(side), j], f_device(half, side)
+            )
 
     def send_second(half, j):
         for side in SIDES:
             block = sum_block(half, side, j)
             rows = sum_rows(block, part_start(half, side), PART)
-            arrived(slot("F1", half, j, side), first1.at[half, which(side), j])
+            arrived(firsts[half, side] + j, first1.at[half, which(side), j])
             add_into(part, rows, [first1[half, which(side), j]])
         for side in SIDES:
             block = sum_block(half, side, j)
@@ -404,68 +417,77 @@
         rows = sum_rows(sum_block(half, 0, j), half * HALF, HALF)
         add_into(part, rows, [first2[half, 0, j], first2[half, 1, j]])
 
-    loop([(2, 2), (2, 1), (2, 3), (2, 0)], finish)
-    for j in (2, 1, 3, 0):
-        send_first(0, j)
-    send_first(1, 2)
-    loop([(1, 2), (3, 2), (0, 2)], finish)
-    for j in (1, 3, 0):
-        send_first(1, j)
+    finish(block_at(2, 2))
+    for half in range(2):
+        send_first(half, 2)
+
+    def outer(n, carried):
+        place = pick(n, (1, 3, 0))
+        finish(block_at(2, place))
+        finish(block_at(place, 2))
+        for half in range(2):
+            send_first(half, place)
+        return carried
+
+    lax.fori_loop(0, 3, outer, 0)
+    for half in range(2):
+        send_second(half, 2)
     loop(corners, finish)
-    for half in range(2):
-        send_second(half, 2)
-    loop([(1, 0), (3, 0), (0, 1), (0, 3), (0, 0)], finish)
-    for j in (1, 3, 0):
+    for j in (1, 3):
         for half in range(2):
             send_second(half, j)
-
-    def weight_part(chunk):
-        columns = pl.ds(pl.multiple_of(chunk * head, head), head)
-        wg[chunk] = t_dot(xall[:, columns], g[...]).astype(BF16)
+    loop([(1, 0), (3, 0), (0, 1), (0, 3), (0, 0)], finish)
 
     ahead = (2, 1, 3, 0)
 
-    def others(n, carried):
-        weight_part(wrap(y + pick(n, ahead)) * 2 + 1 - core)
-        return carried
-
-    lax.fori_loop(0, RING, others, 0)
-    for n in range(RING):
-        chunk = wrap(y + ahead[n]) * 2 + 1 - core
-        send(slot("pair", n), wg.at[chunk], pair1.at[n], partner)
-
-    for half in range(2):
-        take_second(half, 2)
-    for half in range(2):
-        for side in SIDES:
-            rows = sum_rows(sum_block(half, 0, 2), part_start(half, side), PART)
-            send(slot("G1", half, side), part.at[rows, :], second1.at[half, which(side)], g_device(half, side))
-
-    def mine(n, carried):
-        weight_part(wrap(y + pick(n, ahead)) * 2 + core)
-        return carried
-
-    lax.fori_loop(0, RING, mine, 0)
-    for n in range(RING):
+    def weight_parts(n):
+        first = wrap(y + ahead[n]) * 2
+
+        def step(i, carried):
+            chunk = first + jnp.where(i == 0, 1 - core, core)
+            columns = pl.ds(pl.multiple_of(chunk * head, head), head)
+            wg[chunk] = t_dot(xall[:, columns], g[...]).astype(BF16)
+            return carried
+
+        lax.fori_loop(0, 2, step, 0)
+        send(slot("pair", n), wg.at[first + 1 - core], pair1.at[n], partner)
+
+    def add_pair(n):
         chunk = wrap(y + ahead[n]) * 2 + core
         arrived(slot("pair", n), pair1.at[n])
         wg[chunk] = (wg[chunk].astype(F32) + pair1[n].astype(F32)).astype(BF16)
-        if n == 0:
-            for side in SIDES:
-                rows = pl.ds(0 if side == 1 else BLOCK, BLOCK)
-                send(slot("Y1", side), wg.at[chunk, rows, :], ring1.at[which(side)], along_y(side))
-
-    for j in (1, 3):
-        for half in range(2):
-            take_second(half, j)
-
+
+    weight_parts(0)
+    for half in range(2):
+        take_second(half, 2)
+    for half in range(2):
+        for side in SIDES:
+            rows = sum_rows(sum_block(half, 0, 2), part_start(half, side), PART)
+            send(slot("G1", half, side), part.at[rows, :], second1.at[half, which(side)], g_device(half, side))
+    for half in range(2):
+        send_second(half, 0)
+
+    weight_parts(1)
+    add_pair(0)
+    for side in SIDES:
+        chunk = wrap(y + 2) * 2 + core
+        rows = pl.ds(0 if side == 1 else BLOCK, BLOCK)
+        send(slot("Y1", side), wg.at[chunk, rows, :], ring1.at[which(side)], along_y(side))
+    weight_parts(2)
+    add_pair(1)
+    weight_parts(3)
+    add_pair(2)
     for side in SIDES:
         chunk = wrap(y + side) * 2 + core
         rows = pl.ds(0 if side == 1 else BLOCK, BLOCK)
         arrived(slot("Y1", side), ring1.at[which(side)])
         wg[chunk, rows, :] = (wg[chunk, rows, :].astype(F32) + ring1[which(side)].astype(F32)).astype(BF16)
         send(slot("Y2", side), wg.at[chunk], ring2.at[which(side)], along_y(side))
-
+    add_pair(3)
+
+    for j in (1, 3):
+        for half in range(2):
+            take_second(half, j)
     for half in range(2):
         for side in SIDES:
             block = sum_block(half, 0, side)
@@ -479,10 +501,7 @@
 
     for side in SIDES:
         arrived(slot("Y2", side), ring2.at[which(side)])
-    total = (wg[y * 2 + core].astype(F32) + ring2[0].astype(F32) + ring2[1].astype(F32)) * (1.0 / (2 * RING))
-    out_q[...] = total[:, 0:head]
-    out_k[...] = total[:, head : 2 * head]
-    out_v[...] = total[:, 2 * head : 3 * head]
+    out_w[...] = wg[y * 2 + core].astype(F32) + ring2[0].astype(F32) + ring2[1].astype(F32)
 
     for half in range(2):
         for side in SIDES:
@@ -491,12 +510,25 @@
         total = part[rows, :].astype(F32) + second2[half, 0].astype(F32) + second2[half, 1].astype(F32)
         out_x[0, half * HALF : (half + 1) * HALF, :] = total.astype(BF16)
 
+    for half in range(2):
+        for side in SIDES:
+            for j in range(RING):
+                source = first1.at[half, which(side), j]
+                copy(firsts[half, side] + j, source, source, partner).wait_send()
     for index, source in sent:
         copy(index, source, source, partner).wait_send()
 
 
 A2A_ORDER = (1, 15, 4, 12, 3, 5, 11, 13, 2, 14, 8, 6, 7, 9, 10)
 COPIES = 160
+VMEM_LIMIT = 67043328
+
+
+def split_kernel(sum_x, sum_w, out_x, out_q, out_k, out_v):
+    head = out_q.shape[1]
+    out_x[...] = sum_x[...]
+    for place, out in enumerate((out_q, out_k, out_v)):
+        out[...] = sum_w[:, place * head : (place + 1) * head] * (1.0 / (2 * RING))
 
 
 def body(hidden_in, mix_cotangent, query_weight, key_weight, value_weight, decay_log):
@@ -507,16 +539,14 @@
     wide = 3 * head
     vmem = pl.BlockSpec(memory_space=pltpu.VMEM)
     anywhere = pl.BlockSpec(memory_space=pl.ANY)
-    return pl.pallas_call(
+    sum_x, sum_w = pl.pallas_call(
         all_kernel,
         out_shape=(
             jax.ShapeDtypeStruct(hidden_in.shape, BF16),
-            jax.ShapeDtypeStruct((head, head), F32),
-            jax.ShapeDtypeStruct((head, head), F32),
-            jax.ShapeDtypeStruct((head, head), F32),
+            jax.ShapeDtypeStruct((head, wide), F32),
         ),
         in_specs=[pl.BlockSpec(memory_space=pltpu.SMEM)] + [anywhere] * 5,
-        out_specs=(vmem,) * 4,
+        out_specs=(vmem,) * 2,
         scratch_shapes=[
             pltpu.VMEM((length, depth), BF16),
             pltpu.VMEM((depth, wide), BF16),
@@ -546,10 +576,21 @@
             pltpu.SemaphoreType.DMA((COPIES,)),
         ],
         compiler_params=pltpu.CompilerParams(
-            vmem_limit_bytes=67043328, collective_id=0, has_side_effects=True
+            vmem_limit_bytes=VMEM_LIMIT, collective_id=0, has_side_effects=True
         ),
         cost_estimate=pl.CostEstimate(flops=21 * 10**9, bytes_accessed=4 * 10**6, transcendentals=0),
     )(decay_log, hidden_in, mix_cotangent, query_weight, key_weight, value_weight)
+    return pl.pallas_call(
+        split_kernel,
+        out_shape=(
+            jax.ShapeDtypeStruct(hidden_in.shape, BF16),
+            jax.ShapeDtypeStruct((head, head), F32),
+            jax.ShapeDtypeStruct((head, head), F32),
+            jax.ShapeDtypeStruct((head, head), F32),
+        ),
+        in_specs=[vmem] * 2,
+        out_specs=(vmem,) * 4,
+    )(sum_x, sum_w)
 
 
 def solution(mesh):

time: 129 us -> 118 us (0.915)
  Pallas kernels: 123 us -> 117 us
  local copies, waits for them, and re-layouts: 4.72 us -> 0 us
    pallas_call x1, Pallas kernels: 123 us -> 115 us  [body(): pl.pallas_call(all_kernel, out_shape=(jax.ShapeDtypeStruct(hidden_in.shap...]
    unnamed x10 -> x0, local copies, waits for them, and re-layouts: 4.72 us -> none
    pallas_call x0 -> x1, Pallas kernels: none -> 2.36 us  [body(): pl.pallas_call(split_kernel, out_shape=(jax.ShapeDtypeStruct(hidden_in.sh...]
where the time goes in v3:
time: 118 us
  Pallas kernels  117 us (99%)
  between operations  1.29 us (1%)
    pallas_call x1, Pallas kernels, body(): pl.pallas_call(all_kernel, out_shape=(jax.ShapeDtypeStruct(hidden_in.shap...  115 us
    pallas_call x1, Pallas kernels, body(): pl.pallas_call(split_kernel, out_shape=(jax.ShapeDtypeStruct(hidden_in.sh...  2.36 us

profile of v3, /device:TPU:0, one launch (start us, length us, event | category | flops | bytes accessed | tf_op | source)
XLA Modules:
  0.0 118.3 jit_solution(6952523773755652527)
XLA Ops:
  1.3 114.6 %shard_map.93 = (bf16[1,128,2048]{2,1,0:T(8,128)(2,1)}, f32[256,768]{1,0:T(8,128)}) custom-call(f32[1]{0:T(128)S(6)} %copy.10.rate_ref, bf16[1,128,2048]{2,1,0:T(8,128)(2,1)} %own_x.1, bf16[1,128,4096]{2,1,0:T(8,128)(2,1)} %own_cot.1, bf16[256,256]{1,0:T(8,128)(2,1)} %wq_ref.1, bf16[256,256]{1,0:T(8,128)(2,1)} %wk_ref.1, bf16[256,256]{1,0:T(8,128)(2,1)} %wv_ref.1), custom_call_target="tpu_custom_call" | custom-call | flops 20999999488 | bytes 4000000 | tf_op jit(solution)/shard_map/pallas_call | solution.py:542
  115.9 2.4 %shard_map.94 = (bf16[1,128,2048]{2,1,0:T(8,128)(2,1)}, f32[256,256]{1,0:T(8,128)}, f32[256,256]{1,0:T(8,128)}, f32[256,256]{1,0:T(8,128)}) custom-call(bf16[1,128,2048]{2,1,0:T(8,128)(2,1)} %get-tuple-element.6.sum_x, f32[256,768]{1,0:T(8,128)} %get-tuple-element.7.sum_w), custom_call_target="tpu_custom_call" | custom-call | tf_op jit(solution)/shard_map/pallas_call | solution.py:583

commit v4 on v3

--- a/solution.py
+++ b/solution.py
@@ -145,6 +145,10 @@
     local_sem,
     send_sem,
     recv_sem,
+    ready_sem,
+    rate_smem,
+    done_x,
+    done_w,
 ):
     depth = xall.shape[1]
     head = cot.shape[1]
@@ -154,7 +158,6 @@
     dp = lax.axis_index("dp")
     z, x = lax.div(sp, RING), lax.rem(sp, RING)
     y, core = lax.div(dp, 2), lax.rem(dp, 2)
-    rate = rate_ref[0]
     decays = (inner, inner_t, query_d, key_d)
     names = {}
     sent = []
@@ -206,8 +209,8 @@
         copy(index, target, target, partner).wait_recv()
 
     barrier = pltpu.get_barrier_semaphore()
-    friends = [plane(dz, dx) for dz in range(RING) for dx in range(RING) if dz or dx]
-    friends = friends + [along_y(1), along_y(-1), partner]
+    beside = [plane(0, 1), plane(0, -1), plane(1, 0), plane(-1, 0)]
+    friends = beside + [along_y(1), along_y(-1), partner]
     for friend in friends:
         pl.semaphore_signal(barrier, inc=1, device_id=friend, device_id_type=MESH)
 
@@ -222,11 +225,12 @@
             own_cot.at[0, :, pl.ds(pl.multiple_of(sp * head, head), head)], cot.at[own_rows, :], local_sem.at[4]
         ),
     ]
+    loads.append(pltpu.make_async_copy(rate_ref, rate_smem, local_sem.at[5]))
     for load in loads:
         load.start()
-    make_decays(rate, *decays)
     for load in loads:
         load.wait()
+    rate = rate_smem[0]
     pl.semaphore_wait(barrier, len(friends))
 
     def x_rows(block, start, count):
@@ -259,15 +263,24 @@
         first = (wrap(y + dy) * 2 + which) * head
         return w.at[pl.ds(pl.multiple_of(first + start, BLOCK), count), :]
 
-    for half in range(2):
-        for side in SIDES:
-            gather_send(("s1", half, side), half, 0, 0, side, 0)
     for side in SIDES:
         send(slot("w1", side), w_part(0, core, 0, head), w_part(0, core, 0, head), along_y(side))
     send(slot("wc", 0), w_part(0, core, 0, head), w_part(0, core, 0, head), partner)
+
+    @pl.when(core == LATER)
+    def _():
+        pl.semaphore_wait(ready_sem.at[3], 1)
+
+    for half in range(2):
+        for side in SIDES:
+            gather_send(("s1", half, side), half, 0, 0, side, 0)
     for half in range(2):
         for side in SIDES:
             gather_send(("s2", half, 0, side), half, 0, 0, side, 1)
+    for turn in range(3):
+        for friend in beside:
+            pl.semaphore_signal(ready_sem.at[turn], inc=1, device_id=friend, device_id_type=MESH)
+        pl.semaphore_wait(ready_sem.at[turn], len(beside))
     for offset in A2A_ORDER:
         target = lax.rem(sp + offset, blocks)
         send(
@@ -277,6 +290,8 @@
             (target, dp),
         )
 
+    make_decays(rate, *decays)
+
     def project(block):
         rows = rows_of(block)
         got = dot(xall[rows, :], w[...])
@@ -288,13 +303,19 @@
         in_block(block, head, scale, qkv, cot, decays, grads, fwd, bwd)
 
     def loop(places, *works):
+        several = 2 if len(places) % 2 == 0 else 1
+
         def step(n, carried):
-            block = block_at(pick(n, [dz for dz, _ in places]), pick(n, [dx for _, dx in places]))
+            group = []
+            for m in range(several):
+                at = n * several + m
+                group.append(block_at(pick(at, [dz for dz, _ in places]), pick(at, [dx for _, dx in places])))
             for work in works:
-                work(block)
+                for block in group:
+                    work(block)
             return carried
 
-        lax.fori_loop(0, len(places), step, 0)
+        lax.fori_loop(0, len(places) // several, step, 0)
 
     near = [(0, 0), (0, 1), (0, 3), (1, 0), (3, 0)]
     corners = [(1, 1), (1, 3), (3, 1), (3, 3)]
@@ -316,6 +337,10 @@
         send(slot("w2", side), rows, rows, along_y(side))
         rows = w_part(-side, core, 0, head)
         send(slot("wc", side), rows, rows, partner)
+
+    @pl.when(core != LATER)
+    def _():
+        pl.semaphore_signal(ready_sem.at[3], inc=1, device_id=partner, device_id_type=MESH)
 
     for half in range(2):
         for side in SIDES:
@@ -468,12 +493,12 @@
         send_second(half, 0)
 
     weight_parts(1)
+    weight_parts(2)
     add_pair(0)
     for side in SIDES:
         chunk = wrap(y + 2) * 2 + core
         rows = pl.ds(0 if side == 1 else BLOCK, BLOCK)
         send(slot("Y1", side), wg.at[chunk, rows, :], ring1.at[which(side)], along_y(side))
-    weight_parts(2)
     add_pair(1)
     weight_parts(3)
     add_pair(2)
@@ -501,14 +526,20 @@
 
     for side in SIDES:
         arrived(slot("Y2", side), ring2.at[which(side)])
-    out_w[...] = wg[y * 2 + core].astype(F32) + ring2[0].astype(F32) + ring2[1].astype(F32)
+    done_w[...] = wg[y * 2 + core].astype(F32) + ring2[0].astype(F32) + ring2[1].astype(F32)
+    leave_w = pltpu.make_async_copy(done_w, out_w, local_sem.at[6])
+    leave_w.start()
 
     for half in range(2):
         for side in SIDES:
             arrived(slot("G2", half, side), second2.at[half, which(side)])
         rows = sum_rows(sp, half * HALF, HALF)
         total = part[rows, :].astype(F32) + second2[half, 0].astype(F32) + second2[half, 1].astype(F32)
-        out_x[0, half * HALF : (half + 1) * HALF, :] = total.astype(BF16)
+        done_x[half * HALF : (half + 1) * HALF, :] = total.astype(BF16)
+    leave_x = pltpu.make_async_copy(done_x, out_x.at[0], local_sem.at[7])
+    leave_x.start()
+    leave_w.wait()
+    leave_x.wait()
 
     for half in range(2):
         for side in SIDES:
@@ -521,14 +552,28 @@
 
 A2A_ORDER = (1, 15, 4, 12, 3, 5, 11, 13, 2, 14, 8, 6, 7, 9, 10)
 COPIES = 160
+LATER = 1
 VMEM_LIMIT = 67043328
 
 
-def split_kernel(sum_x, sum_w, out_x, out_q, out_k, out_v):
+def split_kernel(sum_x, sum_w, out_x, out_q, out_k, out_v, held_x, held_w, thirds, sems):
     head = out_q.shape[1]
-    out_x[...] = sum_x[...]
+    load_w = pltpu.make_async_copy(sum_w, held_w, sems.at[0])
+    load_x = pltpu.make_async_copy(sum_x, held_x, sems.at[1])
+    load_w.start()
+    load_x.start()
+    load_x.wait()
+    leave_x = pltpu.make_async_copy(held_x, out_x, sems.at[2])
+    leave_x.start()
+    load_w.wait()
+    leaves = [leave_x]
     for place, out in enumerate((out_q, out_k, out_v)):
-        out[...] = sum_w[:, place * head : (place + 1) * head] * (1.0 / (2 * RING))
+        thirds[place] = held_w[:, place * head : (place + 1) * head] * (1.0 / (2 * RING))
+        leave = pltpu.make_async_copy(thirds.at[place], out, sems.at[3 + place])
+        leave.start()
+        leaves.append(leave)
+    for leave in leaves:
+        leave.wait()
 
 
 def body(hidden_in, mix_cotangent, query_weight, key_weight, value_weight, decay_log):
@@ -537,7 +582,6 @@
     blocks = RING * RING
     length = blocks * BLOCK
     wide = 3 * head
-    vmem = pl.BlockSpec(memory_space=pltpu.VMEM)
     anywhere = pl.BlockSpec(memory_space=pl.ANY)
     sum_x, sum_w = pl.pallas_call(
         all_kernel,
@@ -545,8 +589,8 @@
             jax.ShapeDtypeStruct(hidden_in.shape, BF16),
             jax.ShapeDtypeStruct((head, wide), F32),
         ),
-        in_specs=[pl.BlockSpec(memory_space=pltpu.SMEM)] + [anywhere] * 5,
-        out_specs=(vmem,) * 2,
+        in_specs=[pl.BlockSpec(memory_space=pltpu.HBM)] + [anywhere] * 5,
+        out_specs=(anywhere,) * 2,
         scratch_shapes=[
             pltpu.VMEM((length, depth), BF16),
             pltpu.VMEM((depth, wide), BF16),
@@ -571,9 +615,13 @@
             pltpu.VMEM((RING, depth // (2 * RING), wide), BF16),
             pltpu.VMEM((2, depth // (4 * RING), wide), BF16),
             pltpu.VMEM((2, depth // (2 * RING), wide), BF16),
-            pltpu.SemaphoreType.DMA((5,)),
+            pltpu.SemaphoreType.DMA((8,)),
             pltpu.SemaphoreType.DMA((COPIES,)),
             pltpu.SemaphoreType.DMA((COPIES,)),
+            pltpu.SemaphoreType.REGULAR((4,)),
+            pltpu.SMEM((1,), F32),
+            pltpu.VMEM((BLOCK, depth), BF16),
+            pltpu.VMEM((head, wide), F32),
         ],
         compiler_params=pltpu.CompilerParams(
             vmem_limit_bytes=VMEM_LIMIT, collective_id=0, has_side_effects=True
@@ -588,8 +636,14 @@
             jax.ShapeDtypeStruct((head, head), F32),
             jax.ShapeDtypeStruct((head, head), F32),
         ),
-        in_specs=[vmem] * 2,
-        out_specs=(vmem,) * 4,
+        in_specs=[anywhere] * 2,
+        out_specs=(anywhere,) * 4,
+        scratch_shapes=[
+            pltpu.VMEM(hidden_in.shape, BF16),
+            pltpu.VMEM((head, wide), F32),
+            pltpu.VMEM((3, head, head), F32),
+            pltpu.SemaphoreType.DMA((6,)),
+        ],
     )(sum_x, sum_w)
 
 

time: 118 us -> 117 us (level); the launches traced: 118 us -> 115 us
  Pallas kernels: 117 us -> 113 us
    pallas_call x1, Pallas kernels: 115 us -> 111 us  [body(): pl.pallas_call(all_kernel, out_shape=(jax.ShapeDtypeStruct(hidden_in.shap...]
where the time goes in v4:
time: 117 us; the launch traced here: 115 us
  Pallas kernels  113 us (97%)
  between operations  1.45 us (1%)
    pallas_call x1, Pallas kernels, body(): pl.pallas_call(all_kernel, out_shape=(jax.ShapeDtypeStruct(hidden_in.shap...  111 us
    pallas_call x1, Pallas kernels, body(): pl.pallas_call(split_kernel, out_shape=(jax.ShapeDtypeStruct(hidden_in.sh...  2.38 us

profile of v4, /device:TPU:0, one launch (start us, length us, event | category | flops | bytes accessed | tf_op | source)
XLA Modules:
  0.0 114.7 jit_solution(2621884847430002873)
XLA Ops:
  1.3 110.8 %shard_map.93 = (bf16[1,128,2048]{2,1,0:T(8,128)(2,1)}, f32[256,768]{1,0:T(8,128)}) custom-call(f32[1]{0:T(128)S(6)} %copy.10.rate_ref, bf16[1,128,2048]{2,1,0:T(8,128)(2,1)} %own_x.1, bf16[1,128,4096]{2,1,0:T(8,128)(2,1)} %own_cot.1, bf16[256,256]{1,0:T(8,128)(2,1)} %wq_ref.1, bf16[256,256]{1,0:T(8,128)(2,1)} %wk_ref.1, bf16[256,256]{1,0:T(8,128)(2,1)} %wv_ref.1), custom_call_target="tpu_custom_call" | custom-call | flops 20999999488 | bytes 4000000 | tf_op jit(solution)/shard_map/pallas_call | solution.py:586
  112.1 2.4 %shard_map.94 = (bf16[1,128,2048]{2,1,0:T(8,128)(2,1)}, f32[256,256]{1,0:T(8,128)}, f32[256,256]{1,0:T(8,128)}, f32[256,256]{1,0:T(8,128)}) custom-call(bf16[1,128,2048]{2,1,0:T(8,128)(2,1)} %get-tuple-element.6.sum_x, f32[256,768]{1,0:T(8,128)} %get-tuple-element.7.sum_w), custom_call_target="tpu_custom_call" | custom-call | tf_op jit(solution)/shard_map/pallas_call | solution.py:631

commit v5 on v4

--- a/solution.py
+++ b/solution.py
@@ -132,7 +132,6 @@
     bwd,
     fwd_bf,
     bwd_bf,
-    g,
     part,
     first1,
     first2,
@@ -149,6 +148,7 @@
     rate_smem,
     done_x,
     done_w,
+    wt,
 ):
     depth = xall.shape[1]
     head = cot.shape[1]
@@ -355,6 +355,14 @@
 
     loop(near, project)
 
+    def turn_weights(n, carried):
+        rows = pl.ds(pl.multiple_of(n * head, head), head)
+        for third in range(3):
+            wt[third * head : (third + 1) * head, rows] = w[rows, third * head : (third + 1) * head].T
+        return carried
+
+    lax.fori_loop(0, depth // head, turn_weights, 0)
+
     for half in range(2):
         for side in SIDES:
             gather_wait(("f1", half, side), half, 2, 0, side)
@@ -396,10 +404,24 @@
 
     run_states(rate, blocks, fwd, bwd, fwd_bf, bwd_bf)
 
-    def finish(block):
-        cross_block(block, head, scale, qkv, cot, decays, grads, fwd_bf, bwd_bf, g)
-        rows = rows_of(block)
-        part[rows, :] = dot_t(g[rows, :], w[...]).astype(BF16)
+    def finish_all(group):
+        for block in group:
+            cross_block(block, head, scale, qkv, cot, decays, grads, fwd_bf, bwd_bf, qkv)
+        got = jnp.concatenate([qkv[rows_of(block), :] for block in group], axis=0)
+        sums = dot(got, wt[...]).astype(BF16)
+        for place, block in enumerate(group):
+            part[rows_of(block), :] = sums[place * BLOCK : (place + 1) * BLOCK, :]
+
+    def finish_loop(places):
+        def step(n, carried):
+            group = []
+            for m in range(2):
+                at = n * 2 + m
+                group.append(block_at(pick(at, [dz for dz, _ in places]), pick(at, [dx for _, dx in places])))
+            finish_all(group)
+            return carried
+
+        lax.fori_loop(0, len(places) // 2, step, 0)
 
     def sum_block(half, f, q):
         return block_at(*((f, q) if half == 0 else (q, f)))
@@ -442,14 +464,13 @@
         rows = sum_rows(sum_block(half, 0, j), half * HALF, HALF)
         add_into(part, rows, [first2[half, 0, j], first2[half, 1, j]])
 
-    finish(block_at(2, 2))
+    finish_all([block_at(2, 2)])
     for half in range(2):
         send_first(half, 2)
 
     def outer(n, carried):
         place = pick(n, (1, 3, 0))
-        finish(block_at(2, place))
-        finish(block_at(place, 2))
+        finish_all([block_at(2, place), block_at(place, 2)])
         for half in range(2):
             send_first(half, place)
         return carried
@@ -457,11 +478,12 @@
     lax.fori_loop(0, 3, outer, 0)
     for half in range(2):
         send_second(half, 2)
-    loop(corners, finish)
+    finish_loop(corners)
     for j in (1, 3):
         for half in range(2):
             send_second(half, j)
-    loop([(1, 0), (3, 0), (0, 1), (0, 3), (0, 0)], finish)
+    finish_loop([(1, 0), (3, 0), (0, 1), (0, 3)])
+    finish_all([block_at(0, 0)])
 
     ahead = (2, 1, 3, 0)
 
@@ -471,7 +493,7 @@
         def step(i, carried):
             chunk = first + jnp.where(i == 0, 1 - core, core)
             columns = pl.ds(pl.multiple_of(chunk * head, head), head)
-            wg[chunk] = t_dot(xall[:, columns], g[...]).astype(BF16)
+            wg[chunk] = t_dot(xall[:, columns], qkv[...]).astype(BF16)
             return carried
 
         lax.fori_loop(0, 2, step, 0)
@@ -605,7 +627,6 @@
             pltpu.VMEM((blocks, head, head), F32),
             pltpu.VMEM((blocks, head, head), BF16),
             pltpu.VMEM((blocks, head, head), BF16),
-            pltpu.VMEM((length, wide), BF16),
             pltpu.VMEM((length, depth), BF16),
             pltpu.VMEM((2, 2, RING, PART, depth), BF16),
             pltpu.VMEM((2, 2, RING, HALF, depth), BF16),
@@ -622,6 +643,7 @@
             pltpu.SMEM((1,), F32),
             pltpu.VMEM((BLOCK, depth), BF16),
             pltpu.VMEM((head, wide), F32),
+            pltpu.VMEM((wide, depth), BF16),
         ],
         compiler_params=pltpu.CompilerParams(
             vmem_limit_bytes=VMEM_LIMIT, collective_id=0, has_side_effects=True

time: 117 us -> 114 us (0.974)
  Pallas kernels: 113 us -> 110 us
    pallas_call x1, Pallas kernels: 111 us -> 108 us  [body(): pl.pallas_call(all_kernel, out_shape=(jax.ShapeDtypeStruct(hidden_in.shap...]
where the time goes in v5:
time: 114 us; the launch traced here: 112 us
  Pallas kernels  110 us (96%)
  between operations  1.45 us (1%)
    pallas_call x1, Pallas kernels, body(): pl.pallas_call(all_kernel, out_shape=(jax.ShapeDtypeStruct(hidden_in.shap...  108 us
    pallas_call x1, Pallas kernels, body(): pl.pallas_call(split_kernel, out_shape=(jax.ShapeDtypeStruct(hidden_in.sh...  2.38 us

profile of v5, /device:TPU:0, one launch (start us, length us, event | category | flops | bytes accessed | tf_op | source)
XLA Modules:
  0.0 111.9 jit_solution(11472347186329128689)
XLA Ops:
  1.3 108.1 %shard_map.93 = (bf16[1,128,2048]{2,1,0:T(8,128)(2,1)}, f32[256,768]{1,0:T(8,128)}) custom-call(f32[1]{0:T(128)S(6)} %copy.10.rate_ref, bf16[1,128,2048]{2,1,0:T(8,128)(2,1)} %own_x.1, bf16[1,128,4096]{2,1,0:T(8,128)(2,1)} %own_cot.1, bf16[256,256]{1,0:T(8,128)(2,1)} %wq_ref.1, bf16[256,256]{1,0:T(8,128)(2,1)} %wk_ref.1, bf16[256,256]{1,0:T(8,128)(2,1)} %wv_ref.1), custom_call_target="tpu_custom_call" | custom-call | flops 20999999488 | bytes 4000000 | tf_op jit(solution)/shard_map/pallas_call | solution.py:608
  109.3 2.4 %shard_map.94 = (bf16[1,128,2048]{2,1,0:T(8,128)(2,1)}, f32[256,256]{1,0:T(8,128)}, f32[256,256]{1,0:T(8,128)}, f32[256,256]{1,0:T(8,128)}) custom-call(bf16[1,128,2048]{2,1,0:T(8,128)(2,1)} %get-tuple-element.6.sum_x, f32[256,768]{1,0:T(8,128)} %get-tuple-element.7.sum_w), custom_call_target="tpu_custom_call" | custom-call | tf_op jit(solution)/shard_map/pallas_call | solution.py:653

commit v6 on v5

--- a/solution.py
+++ b/solution.py
@@ -574,7 +574,7 @@
 
 A2A_ORDER = (1, 15, 4, 12, 3, 5, 11, 13, 2, 14, 8, 6, 7, 9, 10)
 COPIES = 160
-LATER = 1
+LATER = 0
 VMEM_LIMIT = 67043328
 
 

time: 114 us -> 113 us (level); the launches traced: 112 us -> 113 us
  Pallas kernels: 110 us -> 112 us
    pallas_call x1, Pallas kernels: 108 us -> 109 us  [body(): pl.pallas_call(all_kernel, out_shape=(jax.ShapeDtypeStruct(hidden_in.shap...]
where the time goes in v6:
time: 113 us
  Pallas kernels  112 us (99%)
  between operations  1.45 us (1%)
    pallas_call x1, Pallas kernels, body(): pl.pallas_call(all_kernel, out_shape=(jax.ShapeDtypeStruct(hidden_in.shap...  109 us
    pallas_call x1, Pallas kernels, body(): pl.pallas_call(split_kernel, out_shape=(jax.ShapeDtypeStruct(hidden_in.sh...  2.38 us

profile of v6, /device:TPU:0, one launch (start us, length us, event | category | flops | bytes accessed | tf_op | source)
XLA Modules:
  0.0 113.0 jit_solution(14161609220462260751)
XLA Ops:
  1.3 109.2 %shard_map.93 = (bf16[1,128,2048]{2,1,0:T(8,128)(2,1)}, f32[256,768]{1,0:T(8,128)}) custom-call(f32[1]{0:T(128)S(6)} %copy.10.rate_ref, bf16[1,128,2048]{2,1,0:T(8,128)(2,1)} %own_x.1, bf16[1,128,4096]{2,1,0:T(8,128)(2,1)} %own_cot.1, bf16[256,256]{1,0:T(8,128)(2,1)} %wq_ref.1, bf16[256,256]{1,0:T(8,128)(2,1)} %wk_ref.1, bf16[256,256]{1,0:T(8,128)(2,1)} %wv_ref.1), custom_call_target="tpu_custom_call" | custom-call | flops 20999999488 | bytes 4000000 | tf_op jit(solution)/shard_map/pallas_call | solution.py:608
  110.5 2.4 %shard_map.94 = (bf16[1,128,2048]{2,1,0:T(8,128)(2,1)}, f32[256,256]{1,0:T(8,128)}, f32[256,256]{1,0:T(8,128)}, f32[256,256]{1,0:T(8,128)}) custom-call(bf16[1,128,2048]{2,1,0:T(8,128)(2,1)} %get-tuple-element.6.sum_x, f32[256,768]{1,0:T(8,128)} %get-tuple-element.7.sum_w), custom_call_target="tpu_custom_call" | custom-call | tf_op jit(solution)/shard_map/pallas_call | solution.py:653

commit v7 on v6

--- a/solution.py
+++ b/solution.py
@@ -267,8 +267,26 @@
         send(slot("w1", side), w_part(0, core, 0, head), w_part(0, core, 0, head), along_y(side))
     send(slot("wc", 0), w_part(0, core, 0, head), w_part(0, core, 0, head), partner)
 
+    def exchange():
+        for turn in range(3):
+            for friend in beside:
+                pl.semaphore_signal(ready_sem.at[turn], inc=1, device_id=friend, device_id_type=MESH)
+            pl.semaphore_wait(ready_sem.at[turn], len(beside))
+        for offset in A2A_ORDER:
+            target = lax.rem(sp + offset, blocks)
+            send_in_loop(
+                slot("cot", offset),
+                own_cot.at[0, :, pl.ds(pl.multiple_of(target * head, head), head)],
+                cot.at[own_rows, :],
+                (target, dp),
+            )
+
+    for offset in A2A_ORDER:
+        sent.append((slot("cot", offset), cot.at[0:BLOCK, :]))
+
     @pl.when(core == LATER)
     def _():
+        exchange()
         pl.semaphore_wait(ready_sem.at[3], 1)
 
     for half in range(2):
@@ -277,19 +295,7 @@
     for half in range(2):
         for side in SIDES:
             gather_send(("s2", half, 0, side), half, 0, 0, side, 1)
-    for turn in range(3):
-        for friend in beside:
-            pl.semaphore_signal(ready_sem.at[turn], inc=1, device_id=friend, device_id_type=MESH)
-        pl.semaphore_wait(ready_sem.at[turn], len(beside))
-    for offset in A2A_ORDER:
-        target = lax.rem(sp + offset, blocks)
-        send(
-            slot("cot", offset),
-            own_cot.at[0, :, pl.ds(pl.multiple_of(target * head, head), head)],
-            cot.at[own_rows, :],
-            (target, dp),
-        )
-
+    pl.when(core != LATER)(exchange)
     make_decays(rate, *decays)
 
     def project(block):

time: 113 us -> 116 us (1.027)
  Pallas kernels: 112 us -> 114 us
    pallas_call x1, Pallas kernels: 109 us -> 112 us  [body(): pl.pallas_call(all_kernel, out_shape=(jax.ShapeDtypeStruct(hidden_in.shap...]
where the time goes in v7:
time: 116 us; the launch traced here: 115 us
  Pallas kernels  114 us (98%)
  between operations  1.45 us (1%)
    pallas_call x1, Pallas kernels, body(): pl.pallas_call(all_kernel, out_shape=(jax.ShapeDtypeStruct(hidden_in.shap...  112 us
    pallas_call x1, Pallas kernels, body(): pl.pallas_call(split_kernel, out_shape=(jax.ShapeDtypeStruct(hidden_in.sh...  2.38 us

profile of v7, /device:TPU:0, one launch (start us, length us, event | category | flops | bytes accessed | tf_op | source)
XLA Modules:
  0.0 115.5 jit_solution(3878451446393871884)
XLA Ops:
  1.3 111.6 %shard_map.93 = (bf16[1,128,2048]{2,1,0:T(8,128)(2,1)}, f32[256,768]{1,0:T(8,128)}) custom-call(f32[1]{0:T(128)S(6)} %copy.10.rate_ref, bf16[1,128,2048]{2,1,0:T(8,128)(2,1)} %own_x.1, bf16[1,128,4096]{2,1,0:T(8,128)(2,1)} %own_cot.1, bf16[256,256]{1,0:T(8,128)(2,1)} %wq_ref.1, bf16[256,256]{1,0:T(8,128)(2,1)} %wk_ref.1, bf16[256,256]{1,0:T(8,128)(2,1)} %wv_ref.1), custom_call_target="tpu_custom_call" | custom-call | flops 20999999488 | bytes 4000000 | tf_op jit(solution)/shard_map/pallas_call | solution.py:614
  112.9 2.4 %shard_map.94 = (bf16[1,128,2048]{2,1,0:T(8,128)(2,1)}, f32[256,256]{1,0:T(8,128)}, f32[256,256]{1,0:T(8,128)}, f32[256,256]{1,0:T(8,128)}) custom-call(bf16[1,128,2048]{2,1,0:T(8,128)(2,1)} %get-tuple-element.6.sum_x, f32[256,768]{1,0:T(8,128)} %get-tuple-element.7.sum_w), custom_call_target="tpu_custom_call" | custom-call | tf_op jit(solution)/shard_map/pallas_call | solution.py:659
